TPU v7x, 128 devices: a whole 4x4x4 slice. The times are simulated.
128 devices in a mesh: sp: 16 (over z, x), fs: 4 (over y), tp: 2 (over core).
Axes of the slice: x: 4, y: 4, z: 4, core: 2. Of those that a mesh axis runs over, the one named last changes fastest.
Arguments:
- tokens: bfloat16 [32768, 2048], P(('fs', 'sp')), parts along dimension 0, may hold values from -6 to 6
- norm_gain: bfloat16 [2048], replicated, may hold values from 0.099609375 to 1.8984375
- w_query: bfloat16 [2048, 1024], P('sp', 'tp'), may hold values from -0.15625 to 0.15625
- w_key: bfloat16 [2048, 256], P('sp', 'tp'), may hold values from -0.15625 to 0.15625
- w_value: bfloat16 [2048, 256], P('sp', 'tp'), may hold values from -0.125 to 0.125
- w_glu_value: bfloat16 [2048, 1024], P('sp', 'tp'), may hold values from -0.22097087 to 0.22097087
- w_glu_gate: bfloat16 [2048, 1024], P('sp', 'tp'), may hold values from -0.125 to 0.125
- conv_taps: bfloat16 [31, 1024], P(None, 'tp'), may hold values from -1 to 1
- convolution_norm_gain: bfloat16 [1024], replicated, may hold values from 0.099609375 to 1.8984375
- head_gain: bfloat16 [128], replicated, may hold values from 0.099609375 to 1.8984375
- lam: float32 [8], P('tp'), may hold values from 0.3 to 0.8
- w_out: bfloat16 [2048, 2048], P(None, 'sp'), may hold values from -0.125 to 0.125
Outputs:
- mixed: bfloat16 [32768, 2048], P(('fs', 'sp', 'tp')), parts along dimension 0
- log_totals: float32 [32768, 16], P(('fs', 'sp'), 'tp'), parts along dimension 0
There are 4 independent parts, one for each index of `fs`. A program takes and returns all parts, laid end to end along the dimension named above; an argument that names none is the same for every part. Nothing has to cross between parts.
All inputs are finite; a program needn't handle non-finite values.
Results may differ from a plain program's by a relative error of at most 0.0095.
Values may be sent and summed in bfloat16 or wider, within the bound.
A program may use at most 64 MiB of HBM per device.

v0:
```python
import math

import jax
import jax.numpy as jnp
from jax import lax
from jax.sharding import PartitionSpec as P

HEADS = 8
QK = 64
VDIM = 128
CONV = 1024


def sent_together(arrays, axis, dim, along):
    ends, at = ([], 0)
    for a in arrays[:-1]:
        at += a.shape[along]
        ends.append(at)
    both = jnp.concatenate(arrays, axis=along)
    return tuple(jnp.split(lax.all_gather(both, axis, axis=dim, tiled=True), ends, axis=along))


def from_behind(array, axis, by):
    peers = lax.axis_size(axis)
    pairs = [(i, i + by) for i in range(peers) if 0 <= i + by < peers]
    return lax.ppermute(array, axis, pairs)


def gathered_total(array, axis):
    return lax.all_gather(array, axis).sum(0)


def cut_along(array, dim, peers):
    dims = array.shape
    tiles = array.reshape(*dims[:dim], peers, dims[dim] // peers, *dims[dim + 1 :])
    return jnp.moveaxis(tiles, dim, 0)


def sent_and_summed(array, axis, dim):
    tiles = cut_along(array, dim, lax.axis_size(axis))
    arrived = lax.all_to_all(tiles, axis, split_axis=0, concat_axis=0, tiled=True)
    return arrived.astype(jnp.float32).sum(axis=0)


def body(
    tokens,
    norm_gain,
    w_query,
    w_key,
    w_value,
    w_glu_value,
    w_glu_gate,
    conv_taps,
    convolution_norm_gain,
    head_gain,
    lam,
    w_out,
):
    rows = tokens.shape[0]
    eps = 1e-06
    tok32 = tokens.astype(jnp.float32)
    normalized_rows = (
        tok32
        * lax.rsqrt(jnp.mean(tok32 * tok32, axis=-1, keepdims=True) + eps)
        * norm_gain.astype(jnp.float32)
    ).astype(jnp.bfloat16)
    weights = (w_query, w_key, w_value, w_glu_value, w_glu_gate)
    pieces = sent_together((weights[0], weights[1], weights[2], weights[3], weights[4]), "sp", 0, 1)
    proj = tuple(
        (jnp.dot(normalized_rows, piece, preferred_element_type=jnp.float32) for piece in pieces)
    )
    queries = proj[0].astype(jnp.bfloat16)
    keys = proj[1].astype(jnp.bfloat16)
    values = proj[2].astype(jnp.bfloat16)
    gated = (proj[3] * jax.nn.sigmoid(proj[4])).astype(jnp.bfloat16)
    taps = conv_taps.shape[0]
    rim = from_behind(gated[rows - (taps - 1) :], "sp", 1)
    padded = jnp.concatenate([rim, gated], axis=0)
    conv = jnp.zeros(gated.shape, jnp.float32)
    for tap in range(taps):
        conv = conv + conv_taps[tap].astype(jnp.float32) * padded[tap : tap + rows].astype(
            jnp.float32
        )
    conv_out = conv.astype(jnp.bfloat16)
    heads_here = lam.shape[0]
    kv_here = w_key.shape[1] // (2 * QK)
    group = heads_here // kv_here
    query_view = queries.reshape(rows, kv_here, group, 2, QK)
    query_pos = lax.axis_index("sp") * rows + jnp.arange(rows, dtype=jnp.int32)
    scale = QK ** (-0.5)
    empty = (
        jnp.zeros((rows, kv_here, group, 2, VDIM), jnp.float32),
        jnp.zeros((rows, kv_here, group, 2), jnp.float32),
    )
    key_piece, value_piece = sent_together((keys, values), "sp", 0, 1)
    count = key_piece.shape[0]
    width = math.gcd(count, 512)
    blocks = count // width
    key_blocks = key_piece.reshape(blocks, width, kv_here, 2, QK)
    value_blocks = value_piece.reshape(blocks, width, kv_here, VDIM)

    def step(state, item):
        key_block, value_block, index = item
        score = (
            jnp.einsum(
                "tkgmd,nkmd->tkgmn", query_view, key_block, preferred_element_type=jnp.float32
            )
            * scale
        )
        key_pos = index * width + jnp.arange(width, dtype=jnp.int32)
        allowed = key_pos[None, None, None, None, :] <= query_pos[:, None, None, None, None]
        weight = jnp.where(allowed, jnp.exp(score), 0.0)
        running_total = state[0] + jnp.einsum(
            "doejz,zow->doejw",
            weight.astype(jnp.bfloat16),
            value_block,
            preferred_element_type=jnp.float32,
        )
        total = state[1] + jnp.sum(weight, axis=-1)
        return ((running_total, total), None)

    result, _ = lax.scan(
        step, empty, (key_blocks, value_blocks, jnp.arange(blocks, dtype=jnp.int32))
    )
    running_total, total = result
    running_total = running_total.reshape(rows, heads_here, 2, VDIM)
    total = total.reshape(rows, heads_here, 2)
    diff = (
        running_total[:, :, 0] / total[:, :, 0, None]
        - lam[None, :, None] * running_total[:, :, 1] / total[:, :, 1, None]
    )
    att_out = (
        diff
        * lax.rsqrt(jnp.mean(diff * diff, axis=-1, keepdims=True) + eps)
        * head_gain.astype(jnp.float32)
    )
    att_out = att_out.astype(jnp.bfloat16).reshape(rows, heads_here * VDIM)
    log_totals = jnp.log(total).reshape(rows, heads_here * 2)
    pair_index = lax.axis_index("tp")
    channels_here = conv_out.shape[1]
    att_rows_here = att_out.shape[1]
    conv32 = conv_out.astype(jnp.float32)
    squares = gathered_total(jnp.sum(conv32 * conv32, axis=-1), "tp")
    gain_here = lax.dynamic_slice_in_dim(
        convolution_norm_gain, pair_index * channels_here, channels_here, 0
    ).astype(jnp.float32)
    conv_act = jax.nn.silu(conv32 * lax.rsqrt(squares / CONV + eps)[:, None] * gain_here).astype(
        jnp.bfloat16
    )
    both = jnp.concatenate([att_out, conv_act], axis=1)
    att_weight = lax.dynamic_slice_in_dim(w_out, pair_index * att_rows_here, att_rows_here, 0)
    conv_weight = lax.dynamic_slice_in_dim(
        w_out, HEADS * VDIM + pair_index * channels_here, channels_here, 0
    )
    weight_here = jnp.concatenate([att_weight, conv_weight], axis=0)
    weight_full = lax.all_gather(weight_here, "sp", axis=1, tiled=True)
    mixed = sent_and_summed(
        jnp.dot(both, weight_full, preferred_element_type=jnp.float32).astype(jnp.bfloat16), "tp", 0
    ).astype(jnp.bfloat16)
    return (mixed, log_totals)


def solution(mesh):
    return jax.shard_map(
        body,
        mesh=mesh,
        in_specs=(
            P(("fs", "sp"), None),
            P(),
            P("sp", "tp"),
            P("sp", "tp"),
            P("sp", "tp"),
            P("sp", "tp"),
            P("sp", "tp"),
            P(None, "tp"),
            P(),
            P(),
            P("tp"),
            P(None, "sp"),
        ),
        out_specs=(P(("fs", "sp", "tp"), None), P(("fs", "sp"), "tp")),
        check_vma=False,
    )
```

profile of v0, /device:TPU:1, one launch (start us, length us, event | category | flops | bytes accessed | tf_op | source)
XLA Modules:
  0.0 292.2 jit_solution(7395887095308462581)
XLA Ops:
  15.3 66.6 %all-gather.6.cloned.1.call-done = bf16[2048,1792]{1,0:T(8,128)(2,1)} async-done(((bf16[128,1792]{1,0:T(8,128)(2,1)}), bf16[2048,1792]{1,0:T(8,128)(2,1)}) %all-gather.6.cloned.1.call-update) | async-done | bytes 7340048 | tf_op jit(solution)/shard_map/all_gather | solution.py:20
  87.8 3.8 %fusion.44 = f32[512,512]{1,0:T(8,128)S(1)} fusion(bf16[2048,1792]{1,0:T(8,128)(2,1)} %all-gather.6.cloned.1.call-done, bf16[512,2048]{1,0:T(8,128)(2,1)} %param.14, f32[2048]{0:T(1024)S(1)} %convert_element_type.204, f32[512]{0:T(512)S(1)} %add_rsqrt_fusion.2), kind=kOutput, calls=%fused_computation.69 | convolution fusion | flops 1078722560 | bytes 5253120 | tf_op jit(solution)/shard_map/dot_general | solution.py:70
  91.6 2.9 fusion.41
  94.5 3.1 %collective-permute-start = (bf16[30,512]{1,0:T(8,128)(2,1)S(1)}, bf16[30,512]{1,0:T(8,128)(2,1)S(1)}, u32[]{:S(2)}, u32[]{:S(2)}) collective-permute-start(bf16[30,512]{1,0:T(8,128)(2,1)S(1)} %slice.268), channel_id=1, source_target_pairs={{0,8},{8,16},{16,24},{24,32},{32,40},{40,48},{48,56},{56,64},{64,7... | collective-permute-start | bytes 92168 | tf_op jit(solution)/shard_map/ppermute | solution.py:26
  97.6 3.0 %fusion.38 = bf16[512,512]{0,1:T(8,128)(2,1)S(1)} fusion(bf16[2048,1792]{1,0:T(8,128)(2,1)} %all-gather.6.cloned.1.call-done, bf16[512,2048]{1,0:T(8,128)(2,1)S(1)} %copy-done.2, f32[2048]{0:T(1024)S(1)} %convert_element_type.204, f32[512]{0:T(512)S(1)} %add_rsqrt_fusion.2), kind=kOutput, calls=%fused_computation.67 | convolution fusion | flops 1078198272 | bytes 4728832 | tf_op jit(solution)/shard_map/dot_general | solution.py:70
  101.5 4.6 %fusion.47 = (f32[512]{0:T(512)S(1)}, bf16[512,512]{1,0:T(8,128)(2,1)S(1)}) fusion(bf16[512,512]{1,0:T(8,128)(2,1)S(1)} %fusion.41, f32[512]{0:T(512)S(1)} %bitcast.165, bf16[30,512]{1,0:T(8,128)(2,1)S(1)} %collective-permute-done, f32[512]{0:T(512)S(1)} %bitcast.166, f32[512]{0:T(512)S(1)} %bitcast.168, f32[512]{0:T(512)S(1)} %bitcast.169, ...), kind=kLoop, calls=%fused_computation.72 | loop fusion | flops 48758272 | bytes 1144832 | tf_op jit(solution)/shard_map/reduce_sum | solution.py:143
  106.1 2.8 all-gather.1
  110.1 32.4 %all-gather.8.cloned.1.call-done = bf16[8192,256]{0,1:T(8,128)(2,1)} async-done(((bf16[512,256]{0,1:T(8,128)(2,1)}), bf16[8192,256]{0,1:T(8,128)(2,1)}) %all-gather.8.cloned.1.call-update) | async-done | bytes 4194320 | tf_op jit(solution)/shard_map/all_gather | solution.py:20
  142.5 2.6 fusion.101
  149.4 2.5 copy.24
  151.9 105.9 %while.13 = (s32[]{:T(128)}, f32[512,1,4,2,128]{0,4,3,2,1:T(8,128)S(1)}, f32[512,1,4,2]{0,2,3,1:T(4,128)S(1)}, bf16[16,512,1,128]{1,3,2,0:T(8,128)(2,1)}, s32[16...) while((s32[]{:T(128)}, ...), condition=%wide.region_3.4_spmd.clone, body=%wide.region_1.3_spmd.clone.sunk | while | flops 815010816 | bytes 13967528 | solution.py:122
  153.3 3.1 %fusion.117 = (f32[512,4,2]{0,1,2:T(4,128)S(1)}, bf16[512,4,2,512]{0,3,1,2:T(8,128)(2,1)S(1)}) fusion(pred[512,512]{0,1:T(8,128)(4,1)S(1)} %broadcast_compare_fusion.2, bf16[512,1,4,2,64]{0,4,2,3,1:T(8,128)(2,1)S(1)} %get-tuple-element.241, bf16[16,512,1,2,64]{1,4,3,2,0:T(8,128)(2,1)} %get-tuple-element.240, s32[]{:T(128)S(6)} %copy.60), kind=kOutput, calls=%fused_computation.2.clone.1 | convolution fusion | flops 276819968 | bytes 5128196 | tf_op jit(solution)/shard_map/while/body/eval_jaxpr/tkgmd,nkmd->tkgmn/dot_general | solution.py:105
  160.0 3.1 %fusion.117 = (f32[512,4,2]{0,1,2:T(4,128)S(1)}, bf16[512,4,2,512]{0,3,1,2:T(8,128)(2,1)S(1)}) fusion(pred[512,512]{0,1:T(8,128)(4,1)S(1)} %broadcast_compare_fusion.2, bf16[512,1,4,2,64]{0,4,2,3,1:T(8,128)(2,1)S(1)} %get-tuple-element.241, bf16[16,512,1,2,64]{1,4,3,2,0:T(8,128)(2,1)} %get-tuple-element.240, s32[]{:T(128)S(6)} %copy.60), kind=kOutput, calls=%fused_computation.2.clone.1 | convolution fusion | flops 276819968 | bytes 5128196 | tf_op jit(solution)/shard_map/while/body/eval_jaxpr/tkgmd,nkmd->tkgmn/dot_general | solution.py:105
  166.6 3.1 %fusion.117 = (f32[512,4,2]{0,1,2:T(4,128)S(1)}, bf16[512,4,2,512]{0,3,1,2:T(8,128)(2,1)S(1)}) fusion(pred[512,512]{0,1:T(8,128)(4,1)S(1)} %broadcast_compare_fusion.2, bf16[512,1,4,2,64]{0,4,2,3,1:T(8,128)(2,1)S(1)} %get-tuple-element.241, bf16[16,512,1,2,64]{1,4,3,2,0:T(8,128)(2,1)} %get-tuple-element.240, s32[]{:T(128)S(6)} %copy.60), kind=kOutput, calls=%fused_computation.2.clone.1 | convolution fusion | flops 276819968 | bytes 5128196 | tf_op jit(solution)/shard_map/while/body/eval_jaxpr/tkgmd,nkmd->tkgmn/dot_general | solution.py:105
  173.2 3.1 %fusion.117 = (f32[512,4,2]{0,1,2:T(4,128)S(1)}, bf16[512,4,2,512]{0,3,1,2:T(8,128)(2,1)S(1)}) fusion(pred[512,512]{0,1:T(8,128)(4,1)S(1)} %broadcast_compare_fusion.2, bf16[512,1,4,2,64]{0,4,2,3,1:T(8,128)(2,1)S(1)} %get-tuple-element.241, bf16[16,512,1,2,64]{1,4,3,2,0:T(8,128)(2,1)} %get-tuple-element.240, s32[]{:T(128)S(6)} %copy.60), kind=kOutput, calls=%fused_computation.2.clone.1 | convolution fusion | flops 276819968 | bytes 5128196 | tf_op jit(solution)/shard_map/while/body/eval_jaxpr/tkgmd,nkmd->tkgmn/dot_general | solution.py:105
  179.8 3.1 %fusion.117 = (f32[512,4,2]{0,1,2:T(4,128)S(1)}, bf16[512,4,2,512]{0,3,1,2:T(8,128)(2,1)S(1)}) fusion(pred[512,512]{0,1:T(8,128)(4,1)S(1)} %broadcast_compare_fusion.2, bf16[512,1,4,2,64]{0,4,2,3,1:T(8,128)(2,1)S(1)} %get-tuple-element.241, bf16[16,512,1,2,64]{1,4,3,2,0:T(8,128)(2,1)} %get-tuple-element.240, s32[]{:T(128)S(6)} %copy.60), kind=kOutput, calls=%fused_computation.2.clone.1 | convolution fusion | flops 276819968 | bytes 5128196 | tf_op jit(solution)/shard_map/while/body/eval_jaxpr/tkgmd,nkmd->tkgmn/dot_general | solution.py:105
  186.4 3.1 %fusion.117 = (f32[512,4,2]{0,1,2:T(4,128)S(1)}, bf16[512,4,2,512]{0,3,1,2:T(8,128)(2,1)S(1)}) fusion(pred[512,512]{0,1:T(8,128)(4,1)S(1)} %broadcast_compare_fusion.2, bf16[512,1,4,2,64]{0,4,2,3,1:T(8,128)(2,1)S(1)} %get-tuple-element.241, bf16[16,512,1,2,64]{1,4,3,2,0:T(8,128)(2,1)} %get-tuple-element.240, s32[]{:T(128)S(6)} %copy.60), kind=kOutput, calls=%fused_computation.2.clone.1 | convolution fusion | flops 276819968 | bytes 5128196 | tf_op jit(solution)/shard_map/while/body/eval_jaxpr/tkgmd,nkmd->tkgmn/dot_general | solution.py:105
  193.1 3.1 %fusion.117 = (f32[512,4,2]{0,1,2:T(4,128)S(1)}, bf16[512,4,2,512]{0,3,1,2:T(8,128)(2,1)S(1)}) fusion(pred[512,512]{0,1:T(8,128)(4,1)S(1)} %broadcast_compare_fusion.2, bf16[512,1,4,2,64]{0,4,2,3,1:T(8,128)(2,1)S(1)} %get-tuple-element.241, bf16[16,512,1,2,64]{1,4,3,2,0:T(8,128)(2,1)} %get-tuple-element.240, s32[]{:T(128)S(6)} %copy.60), kind=kOutput, calls=%fused_computation.2.clone.1 | convolution fusion | flops 276819968 | bytes 5128196 | tf_op jit(solution)/shard_map/while/body/eval_jaxpr/tkgmd,nkmd->tkgmn/dot_general | solution.py:105
  199.7 3.1 %fusion.117 = (f32[512,4,2]{0,1,2:T(4,128)S(1)}, bf16[512,4,2,512]{0,3,1,2:T(8,128)(2,1)S(1)}) fusion(pred[512,512]{0,1:T(8,128)(4,1)S(1)} %broadcast_compare_fusion.2, bf16[512,1,4,2,64]{0,4,2,3,1:T(8,128)(2,1)S(1)} %get-tuple-element.241, bf16[16,512,1,2,64]{1,4,3,2,0:T(8,128)(2,1)} %get-tuple-element.240, s32[]{:T(128)S(6)} %copy.60), kind=kOutput, calls=%fused_computation.2.clone.1 | convolution fusion | flops 276819968 | bytes 5128196 | tf_op jit(solution)/shard_map/while/body/eval_jaxpr/tkgmd,nkmd->tkgmn/dot_general | solution.py:105
  206.3 3.1 %fusion.117 = (f32[512,4,2]{0,1,2:T(4,128)S(1)}, bf16[512,4,2,512]{0,3,1,2:T(8,128)(2,1)S(1)}) fusion(pred[512,512]{0,1:T(8,128)(4,1)S(1)} %broadcast_compare_fusion.2, bf16[512,1,4,2,64]{0,4,2,3,1:T(8,128)(2,1)S(1)} %get-tuple-element.241, bf16[16,512,1,2,64]{1,4,3,2,0:T(8,128)(2,1)} %get-tuple-element.240, s32[]{:T(128)S(6)} %copy.60), kind=kOutput, calls=%fused_computation.2.clone.1 | convolution fusion | flops 276819968 | bytes 5128196 | tf_op jit(solution)/shard_map/while/body/eval_jaxpr/tkgmd,nkmd->tkgmn/dot_general | solution.py:105
  212.9 3.1 %fusion.117 = (f32[512,4,2]{0,1,2:T(4,128)S(1)}, bf16[512,4,2,512]{0,3,1,2:T(8,128)(2,1)S(1)}) fusion(pred[512,512]{0,1:T(8,128)(4,1)S(1)} %broadcast_compare_fusion.2, bf16[512,1,4,2,64]{0,4,2,3,1:T(8,128)(2,1)S(1)} %get-tuple-element.241, bf16[16,512,1,2,64]{1,4,3,2,0:T(8,128)(2,1)} %get-tuple-element.240, s32[]{:T(128)S(6)} %copy.60), kind=kOutput, calls=%fused_computation.2.clone.1 | convolution fusion | flops 276819968 | bytes 5128196 | tf_op jit(solution)/shard_map/while/body/eval_jaxpr/tkgmd,nkmd->tkgmn/dot_general | solution.py:105
  219.5 3.1 %fusion.117 = (f32[512,4,2]{0,1,2:T(4,128)S(1)}, bf16[512,4,2,512]{0,3,1,2:T(8,128)(2,1)S(1)}) fusion(pred[512,512]{0,1:T(8,128)(4,1)S(1)} %broadcast_compare_fusion.2, bf16[512,1,4,2,64]{0,4,2,3,1:T(8,128)(2,1)S(1)} %get-tuple-element.241, bf16[16,512,1,2,64]{1,4,3,2,0:T(8,128)(2,1)} %get-tuple-element.240, s32[]{:T(128)S(6)} %copy.60), kind=kOutput, calls=%fused_computation.2.clone.1 | convolution fusion | flops 276819968 | bytes 5128196 | tf_op jit(solution)/shard_map/while/body/eval_jaxpr/tkgmd,nkmd->tkgmn/dot_general | solution.py:105
  226.2 3.1 %fusion.117 = (f32[512,4,2]{0,1,2:T(4,128)S(1)}, bf16[512,4,2,512]{0,3,1,2:T(8,128)(2,1)S(1)}) fusion(pred[512,512]{0,1:T(8,128)(4,1)S(1)} %broadcast_compare_fusion.2, bf16[512,1,4,2,64]{0,4,2,3,1:T(8,128)(2,1)S(1)} %get-tuple-element.241, bf16[16,512,1,2,64]{1,4,3,2,0:T(8,128)(2,1)} %get-tuple-element.240, s32[]{:T(128)S(6)} %copy.60), kind=kOutput, calls=%fused_computation.2.clone.1 | convolution fusion | flops 276819968 | bytes 5128196 | tf_op jit(solution)/shard_map/while/body/eval_jaxpr/tkgmd,nkmd->tkgmn/dot_general | solution.py:105
  232.8 3.1 %fusion.117 = (f32[512,4,2]{0,1,2:T(4,128)S(1)}, bf16[512,4,2,512]{0,3,1,2:T(8,128)(2,1)S(1)}) fusion(pred[512,512]{0,1:T(8,128)(4,1)S(1)} %broadcast_compare_fusion.2, bf16[512,1,4,2,64]{0,4,2,3,1:T(8,128)(2,1)S(1)} %get-tuple-element.241, bf16[16,512,1,2,64]{1,4,3,2,0:T(8,128)(2,1)} %get-tuple-element.240, s32[]{:T(128)S(6)} %copy.60), kind=kOutput, calls=%fused_computation.2.clone.1 | convolution fusion | flops 276819968 | bytes 5128196 | tf_op jit(solution)/shard_map/while/body/eval_jaxpr/tkgmd,nkmd->tkgmn/dot_general | solution.py:105
  239.4 3.1 %fusion.117 = (f32[512,4,2]{0,1,2:T(4,128)S(1)}, bf16[512,4,2,512]{0,3,1,2:T(8,128)(2,1)S(1)}) fusion(pred[512,512]{0,1:T(8,128)(4,1)S(1)} %broadcast_compare_fusion.2, bf16[512,1,4,2,64]{0,4,2,3,1:T(8,128)(2,1)S(1)} %get-tuple-element.241, bf16[16,512,1,2,64]{1,4,3,2,0:T(8,128)(2,1)} %get-tuple-element.240, s32[]{:T(128)S(6)} %copy.60), kind=kOutput, calls=%fused_computation.2.clone.1 | convolution fusion | flops 276819968 | bytes 5128196 | tf_op jit(solution)/shard_map/while/body/eval_jaxpr/tkgmd,nkmd->tkgmn/dot_general | solution.py:105
  246.0 3.1 %fusion.117 = (f32[512,4,2]{0,1,2:T(4,128)S(1)}, bf16[512,4,2,512]{0,3,1,2:T(8,128)(2,1)S(1)}) fusion(pred[512,512]{0,1:T(8,128)(4,1)S(1)} %broadcast_compare_fusion.2, bf16[512,1,4,2,64]{0,4,2,3,1:T(8,128)(2,1)S(1)} %get-tuple-element.241, bf16[16,512,1,2,64]{1,4,3,2,0:T(8,128)(2,1)} %get-tuple-element.240, s32[]{:T(128)S(6)} %copy.60), kind=kOutput, calls=%fused_computation.2.clone.1 | convolution fusion | flops 276819968 | bytes 5128196 | tf_op jit(solution)/shard_map/while/body/eval_jaxpr/tkgmd,nkmd->tkgmn/dot_general | solution.py:105
  252.6 3.1 %fusion.117 = (f32[512,4,2]{0,1,2:T(4,128)S(1)}, bf16[512,4,2,512]{0,3,1,2:T(8,128)(2,1)S(1)}) fusion(pred[512,512]{0,1:T(8,128)(4,1)S(1)} %broadcast_compare_fusion.2, bf16[512,1,4,2,64]{0,4,2,3,1:T(8,128)(2,1)S(1)} %get-tuple-element.241, bf16[16,512,1,2,64]{1,4,3,2,0:T(8,128)(2,1)} %get-tuple-element.240, s32[]{:T(128)S(6)} %copy.60), kind=kOutput, calls=%fused_computation.2.clone.1 | convolution fusion | flops 276819968 | bytes 5128196 | tf_op jit(solution)/shard_map/while/body/eval_jaxpr/tkgmd,nkmd->tkgmn/dot_general | solution.py:105
  261.6 2.5 copy.39
  266.2 2.6 copy.40
  269.4 2.6 fusion.56
  272.0 4.9 %convolution_convert_fusion = bf16[512,2048]{1,0:T(8,128)(2,1)S(1)} fusion(bf16[1024,2048]{1,0:T(8,128)(2,1)} %all-gather.10.cloned.1.call-done, bf16[512,512]{1,0:T(8,128)(2,1)} %fusion.54, bf16[512,512]{1,0:T(8,128)(2,1)} %fusion.56), kind=kOutput, calls=%fused_computation.54 | convolution fusion | flops 2150629376 | bytes 7340032 | tf_op jit(solution)/shard_map/dot_general | solution.py:158
  276.9 7.1 %all_to_all.5 = bf16[2,256,2048]{2,1,0:T(8,128)(2,1)S(1)} all-to-all(bf16[2,256,2048]{2,1,0:T(8,128)(2,1)S(1)} %bitcast.152), channel_id=1, replica_groups=mesh['sp'=16,'fs'=4,'tp'=2] {'tp'}, dimensions={0} | all-to-all | bytes 4194304 | tf_op jit(solution)/shard_map/all_to_all | solution.py:41
  (151 shorter events, 72.8 us)
Async XLA Ops:
  7.2 74.7 %copy-start.1 = (bf16[512,2048]{1,0:T(8,128)(2,1)S(1)}, bf16[512,2048]{1,0:T(8,128)(2,1)}, u32[]{:S(2)}) copy-start(bf16[512,2048]{1,0:T(8,128)(2,1)} %param.14) | copy-start | bytes 6291460
  7.2 74.7 %all-gather.6.cloned.1.call-start = ((), (), s32[]{:S(2)}) async-start(), calls=%async_computation.1 | async-start | bytes 7798784 | tf_op jit(solution)/shard_map/all_gather | solution.py:20
  11.7 0.8 copy-start.3
  12.4 130.1 %all-gather.8.cloned.1.call-start = ((), (), s32[]{:S(2)}) async-start(), calls=%async_computation.2 | async-start | bytes 4456448 | tf_op jit(solution)/shard_map/all_gather | solution.py:20
  83.8 2.9 copy-start.5
  85.8 1.7 copy-start.6
  85.9 1.7 copy-start.9
  85.9 1.8 copy-start.8
  85.9 1.8 copy-start.7
  86.7 185.4 %all-gather.10.cloned.1.call-start = ((), (), s32[]{:S(2)}) async-start(), calls=%async_computation.3 | async-start | bytes 4456448 | tf_op jit(solution)/shard_map/all_gather | solution.py:156
  87.8 3.8 %copy-start.2 = (bf16[512,2048]{1,0:T(8,128)(2,1)S(1)}, bf16[512,2048]{1,0:T(8,128)(2,1)}, u32[]{:S(2)}) copy-start(bf16[512,2048]{1,0:T(8,128)(2,1)} %param.14) | copy-start | bytes 6291460
  94.5 7.0 %collective-permute-start = (bf16[30,512]{1,0:T(8,128)(2,1)S(1)}, bf16[30,512]{1,0:T(8,128)(2,1)S(1)}, u32[]{:S(2)}, u32[]{:S(2)}) collective-permute-start(bf16[30,512]{1,0:T(8,128)(2,1)S(1)} %slice.268), channel_id=1, source_target_pairs={{0,8},{8,16},{16,24},{24,32},{32,40},{40,48},{48,56},{56,64},{64,7... | collective-permute-start | bytes 92168 | tf_op jit(solution)/shard_map/ppermute | solution.py:26
  149.4 2.5 copy-start.4
  265.1 4.3 %copy-start = (f32[512,512]{1,0:T(8,128)S(1)}, f32[512,512]{1,0:T(8,128)}, u32[]{:S(2)}) copy-start(f32[512,512]{1,0:T(8,128)} %copy.39) | copy-start | bytes 3145732
Sparse Core Ops, SparseCore 0:
  12.6 69.2 all-gather.5
  86.8 55.6 all-gather.7
  144.6 56.2 all-gather.9
where the time goes:
time: 294 us; the launch traced here: 292 us
  matrix products  100 us (34%)
  waiting for transfers between devices  99 us (34%)
  local copies, waits for them, and re-layouts  36.1 us (12%)
  other arithmetic  18.6 us (6%)
  between operations  14.1 us (5%)
  loops' own time  11.2 us (4%)
  blocking collectives  9.89 us (3%)
  starting transfers between devices  3.22 us (1%)
    all_gather x2, waiting for transfers between devices, sent_together(): lax.all_gather(both, axis, axis=dim, tiled=True)  99 us
    dot_general x16, matrix products, step(): jnp.einsum('tkgmd,nkmd->tkgmn', query_view, key_block, preferred_element_...  50.1 us
    dot_general x16, matrix products, step(): jnp.einsum('doejz,zow->doejw', weight.astype(jnp.bfloat16), value_block,...  31.4 us
    dot_general x5, matrix products, body(): jnp.dot(normalized_rows, piece, preferred_element_type=jnp.float32)  13.7 us
    unnamed x29, local copies, waits for them, and re-layouts  11.9 us
    another operation x1, loops' own time, body(): lax.scan(step, empty, (key_blocks, value_blocks, jnp.arange(blocks, dtype...  11.2 us
    dynamic_slice x16, local copies, waits for them, and re-layouts, body(): lax.scan(step, empty, (key_blocks, value_blocks, jnp.arange(blocks, dtype...  9.38 us
    all_to_all x1, blocking collectives, sent_and_summed(): lax.all_to_all(tiles, axis, split_axis=0, concat_axis=0, tiled=True)  7.1 us
  transfers between devices with their start and end apart: 4, of which 2 were waited for; matrix products, arithmetic and copies ran while one was open for 47% of the time, Pallas kernels for 0%

commit v1 on v0

v1 whole, which is shorter than its diff:
```python
import functools
import math

import jax
import jax.numpy as jnp
from jax import lax
from jax.experimental import pallas as pl
from jax.experimental.pallas import tpu as pltpu
from jax.sharding import PartitionSpec as P

HEADS = 8
QK = 64
VDIM = 128
CONV = 1024
EPS = 1e-06
RING = 16
ROUNDS = 8
MESH = pl.DeviceIdType.MESH
ANY = pl.BlockSpec(memory_space=pl.ANY)
F32 = jnp.float32
BF16 = jnp.bfloat16


def dot(a, b):
    return jnp.dot(a, b, preferred_element_type=F32)


def place_on(cycle, sp):
    z, x = lax.div(sp, 4), lax.rem(sp, 4)
    lead = z if cycle == 0 else x
    return lead * 4 + lax.rem(z + x, 4)


def member_at(cycle, place):
    place = lax.rem(place + 2 * RING, RING)
    lead = lax.div(place, 4)
    other = lax.rem(lax.rem(place, 4) - lead + 4, 4)
    return lead * 4 + other if cycle == 0 else other * 4 + lead


def kernel(
    tok_hbm, ngain_ref, wq_hbm, wk_hbm, wv_hbm, wgv_hbm, wgg_hbm, taps_ref, cgain_ref, hgain_ref, lam_ref, wout_hbm,
    mixed_ref, logt_ref,
    tok, normed, wa, wg, wo, kv, q, acc, lsum, gpad, conv, squares, both, outbox, inbox, rim_out, sq_in,
    load_sem, send_sem, recv_sem, side_send, side_recv, out_send, out_recv,
):
    rows = tok.shape[0]
    me = lax.axis_index("sp")
    core = lax.axis_index("tp")
    places = [place_on(c, me) for c in range(2)]
    ahead = [member_at(d // 2, places[d // 2] + (1 if d % 2 == 0 else 15)) for d in range(4)]
    after, before = lax.rem(me + 1, RING), lax.rem(me + RING - 1, RING)

    mine = pl.ds(pl.multiple_of(me * 128, 128), 128)
    att_rows = pl.ds(pl.multiple_of(core * 512, 512), 512)
    conv_rows = pl.ds(pl.multiple_of(1024 + core * 512, 512), 512)
    loads = [
        (wk_hbm, wa.at[mine, pl.ds(0, 128)]),
        (wv_hbm, wa.at[mine, pl.ds(128, 128)]),
        (wq_hbm, wa.at[mine, pl.ds(256, 512)]),
        (wgv_hbm, wg.at[mine, pl.ds(0, 512)]),
        (wgg_hbm, wg.at[mine, pl.ds(512, 512)]),
        (tok_hbm, tok),
        (wout_hbm.at[att_rows], wo.at[me, pl.ds(0, 512)]),
        (wout_hbm.at[conv_rows], wo.at[me, pl.ds(512, 512)]),
    ]
    loads = [pltpu.make_async_copy(s, d, load_sem.at[i]) for i, (s, d) in enumerate(loads)]
    for load in loads:
        load.start()

    barrier = pltpu.get_barrier_semaphore()
    for peer in ahead + [after, before]:
        pl.semaphore_signal(barrier, inc=1, device_id={"sp": peer}, device_id_type=MESH)
    pl.semaphore_signal(barrier, inc=1, device_id={"tp": 1 - core}, device_id_type=MESH)
    pl.semaphore_wait(barrier, 7)

    def weight_rows(ref):
        def part(source, cycle, at, size):
            start = source * 128 + cycle * 64 + at * 64 // 2
            return ref.at[pl.ds(pl.multiple_of(start, 32), size * 32)]
        return part

    def out_rows(source, cycle, at, size):
        return wo.at[source, pl.ds(cycle * 512 + at * 256, size * 256)]

    def kv_rows(source, cycle, at, size):
        return kv.at[source * 2 + cycle, pl.ds(at * 256, size * 256)]

    jobs = [weight_rows(wa), weight_rows(wg), kv_rows, out_rows]
    WA, WG, KV, WO = range(4)

    def copy_of(job, d, r, last):
        cycle, way = d // 2, d % 2
        sign = 1 if way == 0 else -1
        source = member_at(cycle, places[cycle] - sign * (r - 1))
        at, size = (way, 1) if last else (0, 2)
        ref = jobs[job](source, cycle, at, size)
        return pltpu.make_async_remote_copy(
            src_ref=ref, dst_ref=ref, send_sem=send_sem.at[job, d, r - 1], recv_sem=recv_sem.at[job, d, r - 1],
            device_id={"sp": ahead[d]}, device_id_type=MESH,
        )

    def arrival_of(job, d, r, last):
        cycle, way = d // 2, d % 2
        sign = 1 if way == 0 else -1
        source = member_at(cycle, places[cycle] - sign * r)
        at, size = (way, 1) if last else (0, 2)
        ref = jobs[job](source, cycle, at, size)
        return pltpu.make_async_remote_copy(
            src_ref=ref, dst_ref=ref, send_sem=send_sem.at[job, d, r - 1], recv_sem=recv_sem.at[job, d, r - 1],
            device_id={"sp": ahead[d]}, device_id_type=MESH,
        )

    def send(job, r, last=False):
        for d in range(4):
            copy_of(job, d, r, last).start()

    def receive(job, r, last=False):
        for d in range(4):
            arrival_of(job, d, r, last).wait_recv()

    def pass_on(job, r, last=False):
        for d in range(4):
            arrival_of(job, d, r, False).wait_recv()
            copy_of(job, d, r + 1, last).start()

    def sent(job):
        def one(r, carry):
            for d in range(4):
                copy_of(job, d, r, False).wait_send()
            return carry
        lax.fori_loop(1, ROUNDS, one, 0)
        for d in range(4):
            copy_of(job, d, ROUNDS, True).wait_send()

    for i in range(3):
        loads[i].wait()
    send(WA, 1)
    for i in range(3, 5):
        loads[i].wait()
    send(WG, 1)
    loads[5].wait()

    def norm_rows(i, carry):
        at = pl.ds(pl.multiple_of(i * 64, 64), 64)
        t = tok[at].astype(F32)
        scale = lax.rsqrt(jnp.mean(t * t, axis=-1, keepdims=True) + EPS)
        normed[at] = (t * scale * ngain_ref[...].astype(F32)).astype(BF16)
        return carry

    lax.fori_loop(0, rows // 64, norm_rows, 0)
    for i in range(6, 8):
        loads[i].wait()

    def weights_round(r, carry):
        pass_on(WA, r)
        pass_on(WG, r)
        return carry

    lax.fori_loop(1, ROUNDS - 1, weights_round, 0)
    pass_on(WA, ROUNDS - 1, True)
    pass_on(WG, ROUNDS - 1, True)
    send(WO, 1)
    receive(WA, ROUNDS, True)

    half = rows // 2
    for c in range(2):
        part = dot(normed[pl.ds(c * half, half)], wa[:, pl.ds(0, 256)])
        keys_t = jnp.transpose(part[:, :128]).astype(BF16)
        kv[me * 2 + c, pl.ds(0, 128)] = keys_t[:, :128]
        kv[me * 2 + c, pl.ds(128, 128)] = keys_t[:, 128:]
        kv[me * 2 + c, pl.ds(256, 256)] = part[:, 128:].astype(BF16)
    send(KV, 1)
    for c in range(2):
        at = pl.ds(c * half, half)
        q[at] = dot(normed[at], wa[:, pl.ds(256, 512)]).astype(BF16)

    receive(WG, ROUNDS, True)

    def gate_rows(i, carry):
        at = pl.ds(pl.multiple_of(i * 256, 256), 256)
        value = dot(normed[at], wg[:, pl.ds(0, 512)])
        gate = dot(normed[at], wg[:, pl.ds(512, 512)])
        gated = (value * jax.nn.sigmoid(gate)).astype(BF16).astype(F32)
        for k in range(4):
            gpad[k, pl.ds(pl.multiple_of(32 + i * 256, 32), 256)] = gated[:, k * 128 : k * 128 + 128]
        return carry

    lax.fori_loop(0, rows // 256, gate_rows, 0)
    for k in range(4):
        rim_out[0, k] = gpad[k, pl.ds(rows, 32)].astype(BF16)
    rim = pltpu.make_async_remote_copy(
        src_ref=rim_out.at[0], dst_ref=rim_out.at[1], send_sem=side_send.at[0], recv_sem=side_recv.at[0],
        device_id={"sp": after}, device_id_type=MESH,
    )
    rim.start()

    c_exp = QK ** (-0.5) * math.log2(math.e)

    def keys_of(piece, m):
        k = kv[piece, pl.ds(0, 256)]
        wide = jnp.concatenate([k[:128], k[128:]], axis=1)
        zero = jnp.zeros((QK, 256), BF16)
        return jnp.concatenate([wide[:QK], zero] if m == 0 else [zero, wide[QK:]], axis=0)

    tile = 256

    def attend(piece, diag, first):
        values = kv[piece, pl.ds(256, 256)]
        keys = [keys_of(piece, m) for m in range(2)]

        def one_head(h, carry):
            columns = pl.ds(pl.multiple_of(h * 128, 128), 128)
            for start in range(0, rows, tile):
                if diag is not None and start + tile <= diag:
                    continue
                at = pl.ds(start, tile)
                queries = q[at, columns]
                for m in range(2):
                    w = jnp.exp2(dot(queries, keys[m]) * c_exp)
                    if diag is not None and start < diag + 255:
                        key_pos = diag + lax.broadcasted_iota(jnp.int32, (tile, 256), 1)
                        row_pos = start + lax.broadcasted_iota(jnp.int32, (tile, 256), 0)
                        w = jnp.where(key_pos <= row_pos, w, 0.0)
                    s = w[:, :128] + w[:, 128:]
                    o = dot(w.astype(BF16), values)
                    if first:
                        lsum[h * 2 + m, at] = s
                        acc[h * 2 + m, at] = o
                    else:
                        lsum[h * 2 + m, at] += s
                        acc[h * 2 + m, at] += o
            return carry

        lax.fori_loop(0, 4, one_head, 0)

    def attend_round(r):
        for d in range(4):
            cycle, way = d // 2, d % 2
            sign = 1 if way == 0 else -1
            source = member_at(cycle, places[cycle] - sign * r)

            @pl.when(source < me)
            def _():
                attend(source * 2 + cycle, None, False)

    attend(me * 2, 0, True)
    attend(me * 2 + 1, 256, False)
    pass_on(KV, 1)
    pass_on(WO, 1)

    rim.wait_recv()
    inside = jnp.where(me > 0, 1.0, 0.0)
    for k in range(4):
        gpad[k, pl.ds(0, 32)] = rim_out[1, k].astype(F32) * inside

    def conv_rows_of(i, carry):
        base = pl.multiple_of(i * 64, 64)
        total = jnp.zeros((64, 128), F32)
        for k in range(4):
            out = jnp.zeros((64, 128), F32)
            window = gpad[k, pl.ds(base, 96)]
            for j in range(31):
                out = out + taps_ref[pl.ds(j, 1), pl.ds(k * 128, 128)] * window[j + 2 : j + 66]
            out = out.astype(BF16).astype(F32)
            conv[pl.ds(base, 64), pl.ds(k * 128, 128)] = out
            total = total + out * out
        squares[pl.ds(base, 64)] = total
        return carry

    lax.fori_loop(0, rows // 64, conv_rows_of, 0)
    sq = pltpu.make_async_remote_copy(
        src_ref=squares, dst_ref=sq_in, send_sem=side_send.at[1], recv_sem=side_recv.at[1],
        device_id={"tp": 1 - core}, device_id_type=MESH,
    )
    sq.start()

    def kv_round(r, carry):
        attend_round(r)
        pass_on(KV, r + 1)
        pass_on(WO, r + 1)
        return carry

    lax.fori_loop(1, ROUNDS - 2, kv_round, 0)
    attend_round(ROUNDS - 2)
    pass_on(KV, ROUNDS - 1, True)
    pass_on(WO, ROUNDS - 1, True)
    attend_round(ROUNDS - 1)

    sq.wait_recv()

    def act_rows(i, carry):
        at = pl.ds(pl.multiple_of(i * 64, 64), 64)
        total = jnp.sum(squares[at] + sq_in[at], axis=-1, keepdims=True)
        gain = cgain_ref[:, pl.ds(pl.multiple_of(core * 512, 512), 512)].astype(F32)
        x = conv[at] * lax.rsqrt(total / CONV + EPS) * gain
        both[at, pl.ds(512, 512)] = (x * jax.nn.sigmoid(x)).astype(BF16)
        return carry

    lax.fori_loop(0, rows // 64, act_rows, 0)

    receive(KV, ROUNDS, True)
    for c in range(2):
        source = member_at(c, places[c] + ROUNDS)

        @pl.when(source < me)
        def _():
            attend(source * 2 + c, None, False)

    def finish_rows(i, carry):
        at = pl.ds(pl.multiple_of(i * 64, 64), 64)
        for h in range(4):
            t0 = jnp.sum(lsum[2 * h, at], axis=-1, keepdims=True)
            t1 = jnp.sum(lsum[2 * h + 1, at], axis=-1, keepdims=True)
            diff = acc[2 * h, at] / t0 - lam_ref[h] * acc[2 * h + 1, at] / t1
            out = diff * lax.rsqrt(jnp.mean(diff * diff, axis=-1, keepdims=True) + EPS) * hgain_ref[...].astype(F32)
            both[at, pl.ds(h * 128, 128)] = out.astype(BF16)
            logt_ref[at, pl.ds(2 * h, 1)] = jnp.log(t0)
            logt_ref[at, pl.ds(2 * h + 1, 1)] = jnp.log(t1)
        return carry

    lax.fori_loop(0, rows // 64, finish_rows, 0)
    receive(WO, ROUNDS, True)

    def out_copy(n):
        return pltpu.make_async_remote_copy(
            src_ref=outbox.at[n], dst_ref=inbox.at[n], send_sem=out_send.at[n], recv_sem=out_recv.at[n],
            device_id={"tp": 1 - core}, device_id_type=MESH,
        )

    theirs = pl.ds(pl.multiple_of((1 - core) * 256, 256), 256)
    ours = pl.ds(pl.multiple_of(core * 256, 256), 256)

    def out_columns(n):
        return jnp.concatenate([wo[2 * n], wo[2 * n + 1]], axis=1)

    def their_part(n, carry):
        outbox[n] = dot(both[theirs], out_columns(n)).astype(BF16)
        out_copy(n).start()
        return carry

    lax.fori_loop(0, 8, their_part, 0)

    def our_part(n, carry):
        part = dot(both[ours], out_columns(n))
        out_copy(n).wait_recv()
        mixed_ref[:, pl.ds(pl.multiple_of(n * 256, 256), 256)] = (part + inbox[n].astype(F32)).astype(BF16)
        return carry

    lax.fori_loop(0, 8, our_part, 0)

    for job in range(4):
        sent(job)
    rim.wait_send()
    sq.wait_send()

    def out_sent(n, carry):
        out_copy(n).wait_send()
        return carry

    lax.fori_loop(0, 8, out_sent, 0)


def body(
    tokens, norm_gain, w_query, w_key, w_value, w_glu_value, w_glu_gate, conv_taps, convolution_norm_gain, head_gain, lam, w_out,
):
    rows = tokens.shape[0]
    d = tokens.shape[1]
    vmem = pl.BlockSpec(memory_space=pltpu.VMEM)
    smem = pl.BlockSpec(memory_space=pltpu.SMEM)
    dma = pltpu.SemaphoreType.DMA
    return pl.pallas_call(
        kernel,
        out_shape=(jax.ShapeDtypeStruct((rows // 2, d), BF16), jax.ShapeDtypeStruct((rows, 8), F32)),
        in_specs=[ANY, vmem, ANY, ANY, ANY, ANY, ANY, vmem, vmem, vmem, smem, ANY],
        out_specs=(vmem, vmem),
        scratch_shapes=[
            pltpu.VMEM((rows, d), BF16),
            pltpu.VMEM((rows, d), BF16),
            pltpu.VMEM((d, 768), BF16),
            pltpu.VMEM((d, 1024), BF16),
            pltpu.VMEM((RING, 1024, 128), BF16),
            pltpu.VMEM((2 * RING, 512, 128), BF16),
            pltpu.VMEM((rows, 512), BF16),
            pltpu.VMEM((8, rows, 128), F32),
            pltpu.VMEM((8, rows, 128), F32),
            pltpu.VMEM((4, rows + 32, 128), F32),
            pltpu.VMEM((rows, 512), F32),
            pltpu.VMEM((rows, 128), F32),
            pltpu.VMEM((rows, 1024), BF16),
            pltpu.VMEM((8, 256, 256), BF16),
            pltpu.VMEM((8, 256, 256), BF16),
            pltpu.VMEM((2, 4, 32, 128), BF16),
            pltpu.VMEM((rows, 128), F32),
            dma((8,)),
            dma((4, 4, ROUNDS)),
            dma((4, 4, ROUNDS)),
            dma((2,)),
            dma((2,)),
            dma((8,)),
            dma((8,)),
        ],
        compiler_params=pltpu.CompilerParams(
            collective_id=0, has_side_effects=True, vmem_limit_bytes=60 * 1024 * 1024
        ),
    )(
        tokens, norm_gain.reshape(1, -1), w_query, w_key, w_value, w_glu_value, w_glu_gate,
        conv_taps.astype(F32), convolution_norm_gain.reshape(1, -1), head_gain.reshape(1, -1), lam, w_out,
    )


def solution(mesh):
    return jax.shard_map(
        body,
        mesh=mesh,
        in_specs=(
            P(("fs", "sp"), None),
            P(),
            P("sp", "tp"),
            P("sp", "tp"),
            P("sp", "tp"),
            P("sp", "tp"),
            P("sp", "tp"),
            P(None, "tp"),
            P(),
            P(),
            P("tp"),
            P(None, "sp"),
        ),
        out_specs=(P(("fs", "sp", "tp"), None), P(("fs", "sp"), "tp")),
        check_vma=False,
    )
```

time: 294 us -> 142 us (0.48)
  the two profiles are of different devices: /device:TPU:1 before, /device:TPU:102 now
where the time goes in v1:
time: 142 us
  Pallas kernels  133 us (94%)
  local copies, waits for them, and re-layouts  6.53 us (5%)
    pallas_call x1, Pallas kernels, body(): pl.pallas_call(kernel, out_shape=(jax.ShapeDtypeStruct((rows // 2, d), BF...  133 us

profile of v1, /device:TPU:102, one launch (start us, length us, event | category | flops | bytes accessed | tf_op | source)
XLA Modules:
  0.0 141.6 jit_solution(6254125750244951847)
XLA Ops:
  0.6 1.3 reshape.14.cgain_ref
  1.9 1.3 reshape.13.ngain_ref
  3.2 1.4 convert_element_type.3.taps_ref
  4.6 133.0 %shard_map.131 = (bf16[256,2048]{1,0:T(8,128)(2,1)}, f32[512,8]{1,0:T(8,128)}) custom-call(bf16[512,2048]{1,0:T(8,128)(2,1)} %tok_hbm.1, bf16[1,2048]{1,0:T(2,128)(2,1)} %reshape.13.ngain_ref, bf16[128,512]{1,0:T(8,128)(2,1)} %wq_hbm.1, bf16[128,128]{1,0:T(8,128)(2,1)} %wk_hbm.1, bf16[128,128]{1,0:T(8,128)(2,1)} %wv_hbm.1, bf16[128,512]{1,0:T(8,128)(2,1)} %wgv_hbm.1, ...), custom_call_target="tpu_custom_call" | custom-call | tf_op jit(solution)/shard_map/pallas_call | solution.py:372
  137.6 1.7 %copy.14 = f32[512,8]{0,1:T(8,128)} copy(f32[512,8]{1,0:T(8,128)} %get-tuple-element.3) | data formatting | bytes 32768 | tf_op jit(solution)/shard_map/pallas_call | solution.py:372
  139.3 2.3 %copy.16 = bf16[256,2048]{1,0:T(8,128)(2,1)} copy(bf16[256,2048]{1,0:T(8,128)(2,1)} %get-tuple-element.6) | data formatting | bytes 2097152

commit v2 on v1

v2 whole, which is shorter than its diff:
```python
import functools
import math

import jax
import jax.numpy as jnp
from jax import lax
from jax.experimental import pallas as pl
from jax.experimental.pallas import tpu as pltpu
from jax.sharding import PartitionSpec as P

HEADS = 8
QK = 64
VDIM = 128
CONV = 1024
EPS = 1e-06
RING = 16
MESH = pl.DeviceIdType.MESH
ANY = pl.BlockSpec(memory_space=pl.ANY)
F32 = jnp.float32
BF16 = jnp.bfloat16


def dot(a, b):
    return jnp.dot(a, b, preferred_element_type=F32)


KINDS = ("u1", "u2", "v0", "vm", "vp", "q0", "q1", "f0", "fm", "fp", "f2")
WAYS = ((0, 1), (1, -1))


def kernel(
    tok_hbm, ngain_ref, wq_hbm, wk_hbm, wv_hbm, wgv_hbm, wgg_hbm, taps_ref, cgain_ref, hgain_ref, lam_ref, wout_hbm,
    mixed_ref, logt_ref,
    tok, normed, wa, wg, wo, kv, q, acc, lsum, gpad, conv, squares, both, outbox, inbox, rim_box, sq_in, taps,
    load_sem, send_sem, recv_sem, plane_send, plane_recv, side_send, side_recv, out_send, out_recv,
):
    rows = tok.shape[0]
    me = lax.axis_index("sp")
    core = lax.axis_index("tp")
    plane = lax.axis_index("fs")
    mine_z, mine_x = lax.div(me, 4), lax.rem(me, 4)
    after, before = lax.rem(me + 1, RING), lax.rem(me + RING - 1, RING)
    planes = [lax.rem(plane + 1, 4), lax.rem(plane + 3, 4)]

    def at_offset(dx, dz):
        return lax.rem(mine_z + dz + 8, 4) * 4 + lax.rem(mine_x + dx + 8, 4)

    def offset(c, du, dv):
        return at_offset(du, dv) if c == 0 else at_offset(dv, du)

    mine = pl.ds(pl.multiple_of(me * 128, 128), 128)
    quarter = pl.ds(pl.multiple_of(plane * 256, 256), 256)
    out_from = lax.div(plane, 2) * 1024 + core * 512 + lax.rem(plane, 2) * 256
    loads = [
        (wk_hbm, wa.at[mine, pl.ds(0, 128)]),
        (wv_hbm, wa.at[mine, pl.ds(128, 128)]),
        (wq_hbm, wa.at[mine, pl.ds(256, 512)]),
        (wout_hbm.at[pl.ds(pl.multiple_of(out_from, 256), 256)], wo.at[me, quarter]),
        (tok_hbm, tok),
        (wgv_hbm, wg.at[mine, pl.ds(0, 512)]),
        (wgg_hbm, wg.at[mine, pl.ds(512, 512)]),
    ]
    loads = [pltpu.make_async_copy(s, d, load_sem.at[i]) for i, (s, d) in enumerate(loads)]
    for load in loads:
        load.start()

    barrier = pltpu.get_barrier_semaphore()
    for peer in [offset(c, s, 0) for c in range(2) for _, s in WAYS] + [after, before]:
        pl.semaphore_signal(barrier, inc=1, device_id={"sp": peer}, device_id_type=MESH)
    for peer in planes:
        pl.semaphore_signal(barrier, inc=1, device_id={"fs": peer}, device_id_type=MESH)
    pl.semaphore_signal(barrier, inc=1, device_id={"tp": 1 - core}, device_id_type=MESH)
    pl.semaphore_wait(barrier, 9)

    def weight_rows(ref):
        def part(source, c, at, size):
            start = source * 128 + c * 64 + at * 32
            return ref.at[pl.ds(pl.multiple_of(start, 32), size * 32)]
        return part

    def out_rows(source, c, at, size):
        start = plane * 256 + c * 128 + at * 64
        return wo.at[source, pl.ds(pl.multiple_of(start, 64), size * 64)]

    def kv_rows(source, c, at, size):
        return kv.at[source * 2 + c, pl.ds(at * 256, size * 256)]

    jobs = [weight_rows(wa), weight_rows(wg), kv_rows, out_rows]
    WA, WG, KV, WO = range(4)

    def message(job, c, w, kind, arriving=False):
        sign = WAYS[w][1]
        along = kind[0] == "u"
        du = {"u1": 0, "u2": -sign, "v0": 0, "f0": 0, "vm": -1, "fm": -1, "vp": 1, "fp": 1, "q0": 2, "q1": 2, "f2": 2}[kind]
        dv = -sign if kind[0] == "f" else 0
        at, size = {"u1": (0, 2), "v0": (0, 2), "vm": (0, 2), "vp": (0, 2), "q0": (0, 1), "q1": (1, 1)}.get(kind, (w, 1))
        peer = offset(c, sign, 0) if along else offset(c, 0, sign)
        if arriving:
            du, dv = (du - sign, dv) if along else (du, dv - sign)
        ref = jobs[job](offset(c, du, dv), c, at, size)
        k = KINDS.index(kind)
        return pltpu.make_async_remote_copy(
            src_ref=ref, dst_ref=ref, send_sem=send_sem.at[job, c, w, k], recv_sem=recv_sem.at[job, c, w, k],
            device_id={"sp": peer}, device_id_type=MESH,
        )

    def go(job, c, w, kind):
        message(job, c, w, kind).start()

    def come(job, c, w, kind):
        message(job, c, w, kind, True).wait_recv()

    BOTH = ((0, 0), (0, 1), (1, 0), (1, 1))

    def step0(job):
        for c, w in BOTH:
            go(job, c, w, "u1")
        for c, w in BOTH:
            go(job, c, w, "v0")

    def step1(job):
        for c, w in BOTH:
            come(job, c, w, "u1")
            go(job, c, w, "u2")
            for w2 in range(2):
                go(job, c, w2, "vm" if w == 0 else "vp")
        for c, w in BOTH:
            come(job, c, w, "v0")
            go(job, c, w, "f0")

    def step2(job):
        for c, w in BOTH:
            come(job, c, w, "u2")
            for w2 in range(2):
                go(job, c, w2, "q0" if w == 0 else "q1")
        for c, w in BOTH:
            for side in "mp":
                come(job, c, w, "v" + side)
                go(job, c, w, "f" + side)
        for c, w in BOTH:
            come(job, c, w, "f0")

    def step3(job):
        for c, w in BOTH:
            come(job, c, w, "q0")
            come(job, c, w, "q1")
            go(job, c, w, "f2")
        for c, w in BOTH:
            come(job, c, w, "fm")
            come(job, c, w, "fp")

    def step4(job):
        for c, w in BOTH:
            come(job, c, w, "f2")

    def plane_message(b, w, forward, arriving=False):
        sign = WAYS[w][1]
        back = (1 if forward else 0) + (1 if arriving else 0)
        quarter = lax.rem(plane - sign * back + 8, 4)
        start = quarter * 256 + (w * 128 if forward else 0)
        ref = wo.at[pl.ds(4 * b, 4), pl.ds(pl.multiple_of(start, 128), 128 if forward else 256)]
        k = 4 * b + 2 * w + (1 if forward else 0)
        return pltpu.make_async_remote_copy(
            src_ref=ref, dst_ref=ref, send_sem=plane_send.at[k], recv_sem=plane_recv.at[k],
            device_id={"fs": planes[w]}, device_id_type=MESH,
        )

    def planes_start():
        for b in range(4):
            for w in range(2):
                plane_message(b, w, False).start()

    def planes_forward(b):
        for w in range(2):
            plane_message(b, w, False, True).wait_recv()
            plane_message(b, w, True).start()

    for i in range(3):
        loads[i].wait()
    step0(WA)
    loads[3].wait()
    step0(WO)
    loads[4].wait()

    def norm_rows(i, carry):
        at = pl.ds(pl.multiple_of(i * 64, 64), 64)
        t = tok[at].astype(F32)
        scale = lax.rsqrt(jnp.mean(t * t, axis=-1, keepdims=True) + EPS)
        normed[at] = (t * scale * ngain_ref[...].astype(F32).reshape(1, -1)).astype(BF16)
        return carry

    step1(WA)
    step1(WO)
    lax.fori_loop(0, rows // 64, norm_rows, 0)
    step2(WA)
    step2(WO)
    step3(WA)
    for i in range(5, 7):
        loads[i].wait()
    step0(WG)
    taps[...] = taps_ref[...].astype(F32)
    step3(WO)
    step4(WA)

    half = rows // 2
    for c in range(2):
        part = dot(normed[pl.ds(c * half, half)], wa[:, pl.ds(0, 256)])
        keys_t = jnp.transpose(part[:, :128]).astype(BF16)
        kv[me * 2 + c, pl.ds(0, 128)] = keys_t[:, :128]
        kv[me * 2 + c, pl.ds(128, 128)] = keys_t[:, 128:]
        kv[me * 2 + c, pl.ds(256, 256)] = part[:, 128:].astype(BF16)
    step0(KV)
    step4(WO)
    planes_start()
    for c in range(2):
        at = pl.ds(c * half, half)
        q[at] = dot(normed[at], wa[:, pl.ds(256, 512)]).astype(BF16)

    c_exp = QK ** (-0.5) * math.log2(math.e)

    def keys_of(pieces, m):
        parts = []
        for piece in pieces:
            k = kv[piece, pl.ds(0, 256)]
            parts += [k[:128], k[128:]]
        wide = jnp.concatenate(parts, axis=1)
        zero = jnp.zeros((QK, wide.shape[1]), BF16)
        return jnp.concatenate([wide[:QK], zero] if m == 0 else [zero, wide[QK:]], axis=0)

    def lane_sum(w):
        s = w[:, :128]
        for k in range(1, w.shape[1] // 128):
            s = s + w[:, k * 128 : k * 128 + 128]
        return s

    def attend_source(source):
        pieces = [source * 2, source * 2 + 1]
        values = jnp.concatenate([kv[p, pl.ds(256, 256)] for p in pieces], axis=0)
        keys = [keys_of(pieces, m) for m in range(2)]
        for h in range(4):
            queries = q[:, pl.ds(h * 128, 128)]
            for m in range(2):
                w = jnp.exp2(dot(queries, keys[m]) * c_exp)
                s = lane_sum(w)
                o = dot(w.astype(BF16), values)
                lsum[h * 2 + m] += s
                acc[h * 2 + m] += o

    def attend_own(c):
        start = c * half
        pieces = [me * 2, me * 2 + 1][: c + 1]
        values = jnp.concatenate([kv[p, pl.ds(256, 256)] for p in pieces], axis=0)
        keys = [keys_of(pieces, m) for m in range(2)]
        at = pl.ds(start, half)
        width = 256 * len(pieces)
        key_pos = lax.broadcasted_iota(jnp.int32, (half, width), 1)
        row_pos = start + lax.broadcasted_iota(jnp.int32, (half, width), 0)
        for h in range(4):
            queries = q[at, pl.ds(h * 128, 128)]
            for m in range(2):
                w = jnp.exp2(dot(queries, keys[m]) * c_exp)
                w = jnp.where(key_pos <= row_pos, w, 0.0)
                lsum[h * 2 + m, at] = lane_sum(w)
                acc[h * 2 + m, at] = dot(w.astype(BF16), values)

    def attend_group(count, where):
        def one(i, carry):
            dx, dz = where(i)
            source = at_offset(dx, dz)

            @pl.when(source < me)
            def _():
                attend_source(source)
            return carry

        lax.fori_loop(0, count, one, 0)

    def odd(i):
        return 1 + 2 * lax.rem(i, 2)

    for c in range(2):
        attend_own(c)
    step1(KV)
    step1(WG)
    attend_group(4, lambda i: ((1 - lax.div(i, 2)) * odd(i), lax.div(i, 2) * odd(i)))
    step2(KV)
    step2(WG)
    planes_forward(0)
    attend_group(4, lambda i: (1 + 2 * lax.div(i, 2), odd(i)))
    step3(KV)
    planes_forward(1)
    attend_group(2, lambda i: (2 * (1 - i), 2 * i))
    step3(WG)
    planes_forward(2)
    attend_group(
        4,
        lambda i: (
            2 * (1 - lax.div(i, 2)) + lax.div(i, 2) * odd(i),
            2 * lax.div(i, 2) + (1 - lax.div(i, 2)) * odd(i),
        ),
    )
    planes_forward(3)

    step4(WG)

    def gate_rows(i, carry):
        at = pl.ds(pl.multiple_of(i * 256, 256), 256)
        value = dot(normed[at], wg[:, pl.ds(0, 512)])
        gate = dot(normed[at], wg[:, pl.ds(512, 512)])
        gated = (value * jax.nn.sigmoid(gate)).astype(BF16).astype(F32)
        for k in range(4):
            gpad[k, pl.ds(pl.multiple_of(32 + i * 256, 32), 256)] = gated[:, k * 128 : k * 128 + 128]
        return carry

    lax.fori_loop(0, rows // 256, gate_rows, 0)
    for k in range(4):
        rim_box[0, k] = gpad[k, pl.ds(rows, 32)].astype(BF16)
    rim = pltpu.make_async_remote_copy(
        src_ref=rim_box.at[0], dst_ref=rim_box.at[1], send_sem=side_send.at[0], recv_sem=side_recv.at[0],
        device_id={"sp": after}, device_id_type=MESH,
    )
    rim.start()

    step4(KV)
    attend_group(1, lambda i: (2, 2))

    def finish_rows(i, carry):
        at = pl.ds(pl.multiple_of(i * 128, 128), 128)
        lane = lax.broadcasted_iota(jnp.int32, (128, 128), 1)
        logs = jnp.zeros((128, 128), F32)
        for h in range(4):
            t0 = jnp.sum(lsum[2 * h, at], axis=-1, keepdims=True)
            t1 = jnp.sum(lsum[2 * h + 1, at], axis=-1, keepdims=True)
            diff = acc[2 * h, at] / t0 - lam_ref[h] * acc[2 * h + 1, at] / t1
            out = diff * lax.rsqrt(jnp.mean(diff * diff, axis=-1, keepdims=True) + EPS) * hgain_ref[...].astype(F32)
            both[at, pl.ds(h * 128, 128)] = out.astype(BF16)
            logs = jnp.where(lane == 2 * h, t0, logs)
            logs = jnp.where(lane == 2 * h + 1, t1, logs)
        logt_ref[:, at] = jnp.log(jnp.transpose(logs)[:8])
        return carry

    lax.fori_loop(0, rows // 128, finish_rows, 0)

    rim.wait_recv()
    inside = jnp.where(me > 0, 1.0, 0.0)
    for k in range(4):
        gpad[k, pl.ds(0, 32)] = rim_box[1, k].astype(F32) * inside

    def conv_rows_of(i, carry):
        base = pl.multiple_of(i * 64, 64)
        total = jnp.zeros((64, 128), F32)
        for k in range(4):
            out = jnp.zeros((64, 128), F32)
            window = gpad[k, pl.ds(base, 96)]
            for j in range(31):
                out = out + taps[pl.ds(j, 1), pl.ds(k * 128, 128)] * window[j + 2 : j + 66]
            out = out.astype(BF16).astype(F32)
            conv[pl.ds(base, 64), pl.ds(k * 128, 128)] = out
            total = total + out * out
        squares[pl.ds(base, 64)] = total
        return carry

    lax.fori_loop(0, rows // 64, conv_rows_of, 0)
    sq = pltpu.make_async_remote_copy(
        src_ref=squares, dst_ref=sq_in, send_sem=side_send.at[1], recv_sem=side_recv.at[1],
        device_id={"tp": 1 - core}, device_id_type=MESH,
    )
    sq.start()
    for b in range(4):
        for w in range(2):
            plane_message(b, w, True, True).wait_recv()
    sq.wait_recv()

    def act_rows(i, carry):
        at = pl.ds(pl.multiple_of(i * 64, 64), 64)
        total = jnp.sum(squares[at] + sq_in[at], axis=-1, keepdims=True)
        gain = cgain_ref[pl.ds(pl.multiple_of(core * 512, 512), 512)].astype(F32).reshape(1, 512)
        x = conv[at] * lax.rsqrt(total / CONV + EPS) * gain
        both[at, pl.ds(512, 512)] = (x * jax.nn.sigmoid(x)).astype(BF16)
        return carry

    lax.fori_loop(0, rows // 64, act_rows, 0)

    def out_copy(n):
        return pltpu.make_async_remote_copy(
            src_ref=outbox.at[n], dst_ref=inbox.at[n], send_sem=out_send.at[n], recv_sem=out_recv.at[n],
            device_id={"tp": 1 - core}, device_id_type=MESH,
        )

    theirs = pl.ds(pl.multiple_of((1 - core) * 256, 256), 256)
    ours = pl.ds(pl.multiple_of(core * 256, 256), 256)

    def out_columns(n):
        return jnp.concatenate([wo[2 * n], wo[2 * n + 1]], axis=1)

    def their_part(n, carry):
        outbox[n] = dot(both[theirs], out_columns(n)).astype(BF16)
        out_copy(n).start()
        return carry

    lax.fori_loop(0, 8, their_part, 0)

    def our_part(n, carry):
        part = dot(both[ours], out_columns(n))
        out_copy(n).wait_recv()
        mixed_ref[:, pl.ds(pl.multiple_of(n * 256, 256), 256)] = (part + inbox[n].astype(F32)).astype(BF16)
        return carry

    lax.fori_loop(0, 8, our_part, 0)

    for job in range(4):
        for c, w in BOTH:
            for kind in KINDS:
                message(job, c, w, kind).wait_send()
    for b in range(4):
        for w in range(2):
            plane_message(b, w, False).wait_send()
            plane_message(b, w, True).wait_send()
    rim.wait_send()
    sq.wait_send()

    def out_sent(n, carry):
        out_copy(n).wait_send()
        return carry

    lax.fori_loop(0, 8, out_sent, 0)


def body(
    tokens, norm_gain, w_query, w_key, w_value, w_glu_value, w_glu_gate, conv_taps, convolution_norm_gain, head_gain, lam, w_out,
):
    rows = tokens.shape[0]
    d = tokens.shape[1]
    vmem = pl.BlockSpec(memory_space=pltpu.VMEM)
    smem = pl.BlockSpec(memory_space=pltpu.SMEM)
    dma = pltpu.SemaphoreType.DMA
    mixed, logs = pl.pallas_call(
        kernel,
        out_shape=(jax.ShapeDtypeStruct((rows // 2, d), BF16), jax.ShapeDtypeStruct((8, rows), F32)),
        in_specs=[ANY, vmem, ANY, ANY, ANY, ANY, ANY, vmem, vmem, vmem, smem, ANY],
        out_specs=(vmem, vmem),
        scratch_shapes=[
            pltpu.VMEM((rows, d), BF16),
            pltpu.VMEM((rows, d), BF16),
            pltpu.VMEM((d, 768), BF16),
            pltpu.VMEM((d, 1024), BF16),
            pltpu.VMEM((RING, 1024, 128), BF16),
            pltpu.VMEM((2 * RING, 512, 128), BF16),
            pltpu.VMEM((rows, 512), BF16),
            pltpu.VMEM((8, rows, 128), F32),
            pltpu.VMEM((8, rows, 128), F32),
            pltpu.VMEM((4, rows + 32, 128), F32),
            pltpu.VMEM((rows, 512), F32),
            pltpu.VMEM((rows, 128), F32),
            pltpu.VMEM((rows, 1024), BF16),
            pltpu.VMEM((8, 256, 256), BF16),
            pltpu.VMEM((8, 256, 256), BF16),
            pltpu.VMEM((2, 4, 32, 128), BF16),
            pltpu.VMEM((rows, 128), F32),
            pltpu.VMEM((31, 512), F32),
            dma((7,)),
            dma((4, 2, 2, len(KINDS))),
            dma((4, 2, 2, len(KINDS))),
            dma((16,)),
            dma((16,)),
            dma((2,)),
            dma((2,)),
            dma((8,)),
            dma((8,)),
        ],
        compiler_params=pltpu.CompilerParams(
            collective_id=0, has_side_effects=True, vmem_limit_bytes=60 * 1024 * 1024
        ),
    )(
        tokens, norm_gain, w_query, w_key, w_value, w_glu_value, w_glu_gate,
        conv_taps, convolution_norm_gain, head_gain.reshape(1, -1), lam, w_out,
    )
    return mixed, logs.T


def solution(mesh):
    return jax.shard_map(
        body,
        mesh=mesh,
        in_specs=(
            P(("fs", "sp"), None),
            P(),
            P("sp", "tp"),
            P("sp", "tp"),
            P("sp", "tp"),
            P("sp", "tp"),
            P("sp", "tp"),
            P(None, "tp"),
            P(),
            P(),
            P("tp"),
            P(None, "sp"),
        ),
        out_specs=(P(("fs", "sp", "tp"), None), P(("fs", "sp"), "tp")),
        check_vma=False,
    )
```

time: 142 us -> 114 us (0.80)
  the two profiles are of different devices: /device:TPU:102 before, /device:TPU:1 now
where the time goes in v2:
time: 114 us
  Pallas kernels  110 us (96%)
  local copies, waits for them, and re-layouts  2.92 us (3%)
    pallas_call x1, Pallas kernels, body(): pl.pallas_call(kernel, out_shape=(jax.ShapeDtypeStruct((rows // 2, d), BF...  110 us
    unnamed x4, local copies, waits for them, and re-layouts  2.92 us

profile of v2, /device:TPU:1, one launch (start us, length us, event | category | flops | bytes accessed | tf_op | source)
XLA Modules:
  0.0 113.7 jit_solution(16293639339142486502)
XLA Ops:
  0.6 110.1 %shard_map.131 = (bf16[256,2048]{1,0:T(8,128)(2,1)}, f32[8,512]{1,0:T(8,128)}) custom-call(bf16[512,2048]{1,0:T(8,128)(2,1)} %tok_hbm.1, bf16[2048]{0:T(1024)(128)(2,1)} %ngain_ref.1, bf16[128,512]{1,0:T(8,128)(2,1)} %wq_hbm.1, bf16[128,128]{1,0:T(8,128)(2,1)} %wk_hbm.1, bf16[128,128]{1,0:T(8,128)(2,1)} %wv_hbm.1, bf16[128,512]{1,0:T(8,128)(2,1)} %wgv_hbm.1, ...), custom_call_target="tpu_custom_call" | custom-call | tf_op jit(solution)/shard_map/pallas_call | solution.py:437
  110.7 0.0 copy-start
  110.7 2.3 %copy.16 = bf16[256,2048]{1,0:T(8,128)(2,1)} copy(bf16[256,2048]{1,0:T(8,128)(2,1)} %get-tuple-element.8) | data formatting | bytes 2097152
  113.1 0.0 copy-done
  113.1 0.6 copy.17
Async XLA Ops:
  110.7 2.3 %copy-start = (f32[8,512]{1,0:T(8,128)S(1)}, f32[8,512]{1,0:T(8,128)}, u32[]{:S(2)}) copy-start(f32[8,512]{1,0:T(8,128)} %get-tuple-element.5) | copy-start | bytes 49156

commit v3 on v2

--- a/solution.py
+++ b/solution.py
@@ -31,7 +31,7 @@
 def kernel(
     tok_hbm, ngain_ref, wq_hbm, wk_hbm, wv_hbm, wgv_hbm, wgg_hbm, taps_ref, cgain_ref, hgain_ref, lam_ref, wout_hbm,
     mixed_ref, logt_ref,
-    tok, normed, wa, wg, wo, kv, q, acc, lsum, gpad, conv, squares, both, outbox, inbox, rim_box, sq_in, taps,
+    tok, normed, wkv, wq, wg, wo, kv, q, acc, lsum, gpad, conv, squares, both, outbox, inbox, rim_box, sq_in, taps,
     load_sem, send_sem, recv_sem, plane_send, plane_recv, side_send, side_recv, out_send, out_recv,
 ):
     rows = tok.shape[0]
@@ -49,16 +49,18 @@
         return at_offset(du, dv) if c == 0 else at_offset(dv, du)
 
     mine = pl.ds(pl.multiple_of(me * 128, 128), 128)
-    quarter = pl.ds(pl.multiple_of(plane * 256, 256), 256)
-    out_from = lax.div(plane, 2) * 1024 + core * 512 + lax.rem(plane, 2) * 256
+    quarter = pl.ds(pl.multiple_of(plane * 128, 128), 128)
+    att_rows = pl.ds(pl.multiple_of(core * 512, 512), 512)
+    conv_rows = pl.ds(pl.multiple_of(1024 + core * 512, 512), 512)
     loads = [
-        (wk_hbm, wa.at[mine, pl.ds(0, 128)]),
-        (wv_hbm, wa.at[mine, pl.ds(128, 128)]),
-        (wq_hbm, wa.at[mine, pl.ds(256, 512)]),
-        (wout_hbm.at[pl.ds(pl.multiple_of(out_from, 256), 256)], wo.at[me, quarter]),
+        (wk_hbm, wkv.at[mine, pl.ds(0, 128)]),
+        (wv_hbm, wkv.at[mine, pl.ds(128, 128)]),
+        (wq_hbm, wq.at[mine]),
+        (wgv_hbm.at[:, quarter], wg.at[plane, 0, mine]),
+        (wgg_hbm.at[:, quarter], wg.at[plane, 1, mine]),
         (tok_hbm, tok),
-        (wgv_hbm, wg.at[mine, pl.ds(0, 512)]),
-        (wgg_hbm, wg.at[mine, pl.ds(512, 512)]),
+        (wout_hbm.at[att_rows], wo.at[me, pl.ds(0, 512)]),
+        (wout_hbm.at[conv_rows], wo.at[me, pl.ds(512, 512)]),
     ]
     loads = [pltpu.make_async_copy(s, d, load_sem.at[i]) for i, (s, d) in enumerate(loads)]
     for load in loads:
@@ -78,15 +80,20 @@
             return ref.at[pl.ds(pl.multiple_of(start, 32), size * 32)]
         return part
 
-    def out_rows(source, c, at, size):
-        start = plane * 256 + c * 128 + at * 64
-        return wo.at[source, pl.ds(pl.multiple_of(start, 64), size * 64)]
+    def glu_rows(source, c, at, size):
+        start = source * 128 + c * 64 + at * 32
+        return wg.at[plane, :, pl.ds(pl.multiple_of(start, 32), size * 32)]
+
+    def out_rows(first):
+        def part(source, c, at, size):
+            return wo.at[source, pl.ds(first + c * 256 + at * 128, size * 128)]
+        return part
 
     def kv_rows(source, c, at, size):
         return kv.at[source * 2 + c, pl.ds(at * 256, size * 256)]
 
-    jobs = [weight_rows(wa), weight_rows(wg), kv_rows, out_rows]
-    WA, WG, KV, WO = range(4)
+    jobs = [weight_rows(wkv), weight_rows(wq), glu_rows, kv_rows, out_rows(0), out_rows(512)]
+    WKV, WQ, WG, KV, WOA, WOB = range(6)
 
     def message(job, c, w, kind, arriving=False):
         sign = WAYS[w][1]
@@ -156,9 +163,9 @@
     def plane_message(b, w, forward, arriving=False):
         sign = WAYS[w][1]
         back = (1 if forward else 0) + (1 if arriving else 0)
-        quarter = lax.rem(plane - sign * back + 8, 4)
-        start = quarter * 256 + (w * 128 if forward else 0)
-        ref = wo.at[pl.ds(4 * b, 4), pl.ds(pl.multiple_of(start, 128), 128 if forward else 256)]
+        owner = lax.rem(plane - sign * back + 8, 4)
+        start = b * 512 + (w * 256 if forward else 0)
+        ref = wg.at[owner, :, pl.ds(start, 256 if forward else 512)]
         k = 4 * b + 2 * w + (1 if forward else 0)
         return pltpu.make_async_remote_copy(
             src_ref=ref, dst_ref=ref, send_sem=plane_send.at[k], recv_sem=plane_recv.at[k],
@@ -175,12 +182,7 @@
             plane_message(b, w, False, True).wait_recv()
             plane_message(b, w, True).start()
 
-    for i in range(3):
-        loads[i].wait()
-    step0(WA)
-    loads[3].wait()
-    step0(WO)
-    loads[4].wait()
+    half = rows // 2
 
     def norm_rows(i, carry):
         at = pl.ds(pl.multiple_of(i * 64, 64), 64)
@@ -188,33 +190,6 @@
         scale = lax.rsqrt(jnp.mean(t * t, axis=-1, keepdims=True) + EPS)
         normed[at] = (t * scale * ngain_ref[...].astype(F32).reshape(1, -1)).astype(BF16)
         return carry
-
-    step1(WA)
-    step1(WO)
-    lax.fori_loop(0, rows // 64, norm_rows, 0)
-    step2(WA)
-    step2(WO)
-    step3(WA)
-    for i in range(5, 7):
-        loads[i].wait()
-    step0(WG)
-    taps[...] = taps_ref[...].astype(F32)
-    step3(WO)
-    step4(WA)
-
-    half = rows // 2
-    for c in range(2):
-        part = dot(normed[pl.ds(c * half, half)], wa[:, pl.ds(0, 256)])
-        keys_t = jnp.transpose(part[:, :128]).astype(BF16)
-        kv[me * 2 + c, pl.ds(0, 128)] = keys_t[:, :128]
-        kv[me * 2 + c, pl.ds(128, 128)] = keys_t[:, 128:]
-        kv[me * 2 + c, pl.ds(256, 256)] = part[:, 128:].astype(BF16)
-    step0(KV)
-    step4(WO)
-    planes_start()
-    for c in range(2):
-        at = pl.ds(c * half, half)
-        q[at] = dot(normed[at], wa[:, pl.ds(256, 512)]).astype(BF16)
 
     c_exp = QK ** (-0.5) * math.log2(math.e)
 
@@ -263,7 +238,7 @@
                 lsum[h * 2 + m, at] = lane_sum(w)
                 acc[h * 2 + m, at] = dot(w.astype(BF16), values)
 
-    def attend_group(count, where):
+    def attend_group(first, count, where):
         def one(i, carry):
             dx, dz = where(i)
             source = at_offset(dx, dz)
@@ -273,56 +248,37 @@
                 attend_source(source)
             return carry
 
-        lax.fori_loop(0, count, one, 0)
+        lax.fori_loop(first, first + count, one, 0)
 
     def odd(i):
         return 1 + 2 * lax.rem(i, 2)
 
-    for c in range(2):
-        attend_own(c)
-    step1(KV)
-    step1(WG)
-    attend_group(4, lambda i: ((1 - lax.div(i, 2)) * odd(i), lax.div(i, 2) * odd(i)))
-    step2(KV)
-    step2(WG)
-    planes_forward(0)
-    attend_group(4, lambda i: (1 + 2 * lax.div(i, 2), odd(i)))
-    step3(KV)
-    planes_forward(1)
-    attend_group(2, lambda i: (2 * (1 - i), 2 * i))
-    step3(WG)
-    planes_forward(2)
-    attend_group(
-        4,
-        lambda i: (
-            2 * (1 - lax.div(i, 2)) + lax.div(i, 2) * odd(i),
-            2 * lax.div(i, 2) + (1 - lax.div(i, 2)) * odd(i),
-        ),
-    )
-    planes_forward(3)
-
-    step4(WG)
+    def straight(i):
+        return (1 - lax.div(i, 2)) * odd(i), lax.div(i, 2) * odd(i)
+
+    def corner(i):
+        return 1 + 2 * lax.div(i, 2), odd(i)
+
+    def opposite(i):
+        return 2 * (1 - i), 2 * i
+
+    def knight(i):
+        side = lax.div(i, 2)
+        return 2 * (1 - side) + side * odd(i), 2 * side + (1 - side) * odd(i)
 
     def gate_rows(i, carry):
         at = pl.ds(pl.multiple_of(i * 256, 256), 256)
-        value = dot(normed[at], wg[:, pl.ds(0, 512)])
-        gate = dot(normed[at], wg[:, pl.ds(512, 512)])
+        value = dot(normed[at], jnp.concatenate([wg[k, 0] for k in range(4)], axis=1))
+        gate = dot(normed[at], jnp.concatenate([wg[k, 1] for k in range(4)], axis=1))
         gated = (value * jax.nn.sigmoid(gate)).astype(BF16).astype(F32)
         for k in range(4):
             gpad[k, pl.ds(pl.multiple_of(32 + i * 256, 32), 256)] = gated[:, k * 128 : k * 128 + 128]
         return carry
 
-    lax.fori_loop(0, rows // 256, gate_rows, 0)
-    for k in range(4):
-        rim_box[0, k] = gpad[k, pl.ds(rows, 32)].astype(BF16)
     rim = pltpu.make_async_remote_copy(
         src_ref=rim_box.at[0], dst_ref=rim_box.at[1], send_sem=side_send.at[0], recv_sem=side_recv.at[0],
         device_id={"sp": after}, device_id_type=MESH,
     )
-    rim.start()
-
-    step4(KV)
-    attend_group(1, lambda i: (2, 2))
 
     def finish_rows(i, carry):
         at = pl.ds(pl.multiple_of(i * 128, 128), 128)
@@ -339,12 +295,6 @@
         logt_ref[:, at] = jnp.log(jnp.transpose(logs)[:8])
         return carry
 
-    lax.fori_loop(0, rows // 128, finish_rows, 0)
-
-    rim.wait_recv()
-    inside = jnp.where(me > 0, 1.0, 0.0)
-    for k in range(4):
-        gpad[k, pl.ds(0, 32)] = rim_box[1, k].astype(F32) * inside
 
     def conv_rows_of(i, carry):
         base = pl.multiple_of(i * 64, 64)
@@ -360,16 +310,10 @@
         squares[pl.ds(base, 64)] = total
         return carry
 
-    lax.fori_loop(0, rows // 64, conv_rows_of, 0)
     sq = pltpu.make_async_remote_copy(
         src_ref=squares, dst_ref=sq_in, send_sem=side_send.at[1], recv_sem=side_recv.at[1],
         device_id={"tp": 1 - core}, device_id_type=MESH,
     )
-    sq.start()
-    for b in range(4):
-        for w in range(2):
-            plane_message(b, w, True, True).wait_recv()
-    sq.wait_recv()
 
     def act_rows(i, carry):
         at = pl.ds(pl.multiple_of(i * 64, 64), 64)
@@ -379,8 +323,6 @@
         both[at, pl.ds(512, 512)] = (x * jax.nn.sigmoid(x)).astype(BF16)
         return carry
 
-    lax.fori_loop(0, rows // 64, act_rows, 0)
-
     def out_copy(n):
         return pltpu.make_async_remote_copy(
             src_ref=outbox.at[n], dst_ref=inbox.at[n], send_sem=out_send.at[n], recv_sem=out_recv.at[n],
@@ -391,24 +333,98 @@
     ours = pl.ds(pl.multiple_of(core * 256, 256), 256)
 
     def out_columns(n):
-        return jnp.concatenate([wo[2 * n], wo[2 * n + 1]], axis=1)
-
-    def their_part(n, carry):
+        return jnp.concatenate([wo[8 * n + k] for k in range(8)], axis=1)
+
+    loads[0].wait()
+    loads[1].wait()
+    step0(WKV)
+    loads[3].wait()
+    loads[4].wait()
+    step0(WG)
+    loads[5].wait()
+    lax.fori_loop(0, rows // 64, norm_rows, 0)
+    taps[...] = taps_ref[...].astype(F32)
+    loads[2].wait()
+    step0(WQ)
+    step1(WKV)
+    step1(WG)
+    step2(WKV)
+    step1(WQ)
+    step3(WKV)
+    step2(WG)
+    step2(WQ)
+    step4(WKV)
+    for c in range(2):
+        part = dot(normed[pl.ds(c * half, half)], wkv[...])
+        keys_t = jnp.transpose(part[:, :128]).astype(BF16)
+        kv[me * 2 + c, pl.ds(0, 128)] = keys_t[:, :128]
+        kv[me * 2 + c, pl.ds(128, 128)] = keys_t[:, 128:]
+        kv[me * 2 + c, pl.ds(256, 256)] = part[:, 128:].astype(BF16)
+    step3(WG)
+    step3(WQ)
+    step0(KV)
+    step4(WG)
+    planes_start()
+    step4(WQ)
+    for c in range(2):
+        at = pl.ds(c * half, half)
+        q[at] = dot(normed[at], wq[...]).astype(BF16)
+    for c in range(2):
+        attend_own(c)
+    step1(KV)
+    loads[6].wait()
+    step0(WOA)
+    attend_group(0, 2, straight)
+    loads[7].wait()
+    step0(WOB)
+    attend_group(2, 2, straight)
+    step2(KV)
+    attend_group(0, 2, corner)
+    planes_forward(0)
+    planes_forward(1)
+    step1(WOA)
+    attend_group(2, 2, corner)
+    step1(WOB)
+    planes_forward(2)
+    planes_forward(3)
+    attend_group(0, 2, opposite)
+    step3(KV)
+    attend_group(0, 2, knight)
+    for b in range(4):
+        for w in range(2):
+            plane_message(b, w, True, True).wait_recv()
+    step2(WOB)
+    step2(WOA)
+    lax.fori_loop(0, rows // 256, gate_rows, 0)
+    for k in range(4):
+        rim_box[0, k] = gpad[k, pl.ds(rows, 32)].astype(BF16)
+    rim.start()
+    attend_group(2, 2, knight)
+    step4(KV)
+    rim.wait_recv()
+    step3(WOB)
+    inside = jnp.where(me > 0, 1.0, 0.0)
+    for k in range(4):
+        gpad[k, pl.ds(0, 32)] = rim_box[1, k].astype(F32) * inside
+
+    lax.fori_loop(0, rows // 64, conv_rows_of, 0)
+    sq.start()
+    attend_group(0, 1, lambda i: (2, 2))
+    step3(WOA)
+    lax.fori_loop(0, rows // 128, finish_rows, 0)
+    sq.wait_recv()
+    lax.fori_loop(0, rows // 64, act_rows, 0)
+    step4(WOB)
+    step4(WOA)
+    for n in range(2):
         outbox[n] = dot(both[theirs], out_columns(n)).astype(BF16)
         out_copy(n).start()
-        return carry
-
-    lax.fori_loop(0, 8, their_part, 0)
-
-    def our_part(n, carry):
+    for n in range(2):
         part = dot(both[ours], out_columns(n))
         out_copy(n).wait_recv()
-        mixed_ref[:, pl.ds(pl.multiple_of(n * 256, 256), 256)] = (part + inbox[n].astype(F32)).astype(BF16)
-        return carry
-
-    lax.fori_loop(0, 8, our_part, 0)
-
-    for job in range(4):
+        mixed_ref[:, pl.ds(n * 1024, 1024)] = (part + inbox[n].astype(F32)).astype(BF16)
+
+    for job in range(6):
         for c, w in BOTH:
             for kind in KINDS:
                 message(job, c, w, kind).wait_send()
@@ -419,11 +435,8 @@
     rim.wait_send()
     sq.wait_send()
 
-    def out_sent(n, carry):
+    for n in range(2):
         out_copy(n).wait_send()
-        return carry
-
-    lax.fori_loop(0, 8, out_sent, 0)
 
 
 def body(
@@ -442,8 +455,9 @@
         scratch_shapes=[
             pltpu.VMEM((rows, d), BF16),
             pltpu.VMEM((rows, d), BF16),
-            pltpu.VMEM((d, 768), BF16),
-            pltpu.VMEM((d, 1024), BF16),
+            pltpu.VMEM((d, 256), BF16),
+            pltpu.VMEM((d, 512), BF16),
+            pltpu.VMEM((4, 2, d, 128), BF16),
             pltpu.VMEM((RING, 1024, 128), BF16),
             pltpu.VMEM((2 * RING, 512, 128), BF16),
             pltpu.VMEM((rows, 512), BF16),
@@ -453,20 +467,20 @@
             pltpu.VMEM((rows, 512), F32),
             pltpu.VMEM((rows, 128), F32),
             pltpu.VMEM((rows, 1024), BF16),
-            pltpu.VMEM((8, 256, 256), BF16),
-            pltpu.VMEM((8, 256, 256), BF16),
+            pltpu.VMEM((2, 256, 1024), BF16),
+            pltpu.VMEM((2, 256, 1024), BF16),
             pltpu.VMEM((2, 4, 32, 128), BF16),
             pltpu.VMEM((rows, 128), F32),
             pltpu.VMEM((31, 512), F32),
-            dma((7,)),
-            dma((4, 2, 2, len(KINDS))),
-            dma((4, 2, 2, len(KINDS))),
+            dma((8,)),
+            dma((6, 2, 2, len(KINDS))),
+            dma((6, 2, 2, len(KINDS))),
             dma((16,)),
             dma((16,)),
             dma((2,)),
             dma((2,)),
-            dma((8,)),
-            dma((8,)),
+            dma((2,)),
+            dma((2,)),
         ],
         compiler_params=pltpu.CompilerParams(
             collective_id=0, has_side_effects=True, vmem_limit_bytes=60 * 1024 * 1024

time: 114 us -> 99.6 us (0.87)
  Pallas kernels: 110 us -> 95.9 us
    pallas_call x1, Pallas kernels: 110 us -> 95.9 us  [body(): pl.pallas_call(kernel, out_shape=(jax.ShapeDtypeStruct((rows // 2, d), BF...]
where the time goes in v3:
time: 99.6 us; the launch traced here: 99.4 us
  Pallas kernels  95.9 us (96%)
  local copies, waits for them, and re-layouts  2.92 us (3%)
    pallas_call x1, Pallas kernels, body(): pl.pallas_call(kernel, out_shape=(jax.ShapeDtypeStruct((rows // 2, d), BF...  95.9 us
    unnamed x4, local copies, waits for them, and re-layouts  2.92 us

profile of v3, /device:TPU:1, one launch (start us, length us, event | category | flops | bytes accessed | tf_op | source)
XLA Modules:
  0.0 99.4 jit_solution(7359231023942960835)
XLA Ops:
  0.6 95.9 %shard_map.131 = (bf16[256,2048]{1,0:T(8,128)(2,1)}, f32[8,512]{1,0:T(8,128)}) custom-call(bf16[512,2048]{1,0:T(8,128)(2,1)} %tok_hbm.1, bf16[2048]{0:T(1024)(128)(2,1)} %ngain_ref.1, bf16[128,512]{1,0:T(8,128)(2,1)} %wq_hbm.1, bf16[128,128]{1,0:T(8,128)(2,1)} %wk_hbm.1, bf16[128,128]{1,0:T(8,128)(2,1)} %wv_hbm.1, bf16[128,512]{1,0:T(8,128)(2,1)} %wgv_hbm.1, ...), custom_call_target="tpu_custom_call" | custom-call | tf_op jit(solution)/shard_map/pallas_call | solution.py:450
  96.5 0.0 copy-start
  96.5 2.3 %copy.16 = bf16[256,2048]{1,0:T(8,128)(2,1)} copy(bf16[256,2048]{1,0:T(8,128)(2,1)} %get-tuple-element.8) | data formatting | bytes 2097152
  98.8 0.0 copy-done
  98.8 0.6 copy.17
Async XLA Ops:
  96.5 2.3 %copy-start = (f32[8,512]{1,0:T(8,128)S(1)}, f32[8,512]{1,0:T(8,128)}, u32[]{:S(2)}) copy-start(f32[8,512]{1,0:T(8,128)} %get-tuple-element.5) | copy-start | bytes 49156

commit v4 on v3

--- a/solution.py
+++ b/solution.py
@@ -266,14 +266,12 @@
         side = lax.div(i, 2)
         return 2 * (1 - side) + side * odd(i), 2 * side + (1 - side) * odd(i)
 
-    def gate_rows(i, carry):
-        at = pl.ds(pl.multiple_of(i * 256, 256), 256)
-        value = dot(normed[at], jnp.concatenate([wg[k, 0] for k in range(4)], axis=1))
-        gate = dot(normed[at], jnp.concatenate([wg[k, 1] for k in range(4)], axis=1))
+    def gate_rows():
+        value = dot(normed[...], jnp.concatenate([wg[k, 0] for k in range(4)], axis=1))
+        gate = dot(normed[...], jnp.concatenate([wg[k, 1] for k in range(4)], axis=1))
         gated = (value * jax.nn.sigmoid(gate)).astype(BF16).astype(F32)
         for k in range(4):
-            gpad[k, pl.ds(pl.multiple_of(32 + i * 256, 32), 256)] = gated[:, k * 128 : k * 128 + 128]
-        return carry
+            gpad[k, pl.ds(32, rows)] = gated[:, k * 128 : k * 128 + 128]
 
     rim = pltpu.make_async_remote_copy(
         src_ref=rim_box.at[0], dst_ref=rim_box.at[1], send_sem=side_send.at[0], recv_sem=side_recv.at[0],
@@ -301,9 +299,8 @@
         total = jnp.zeros((64, 128), F32)
         for k in range(4):
             out = jnp.zeros((64, 128), F32)
-            window = gpad[k, pl.ds(base, 96)]
             for j in range(31):
-                out = out + taps[pl.ds(j, 1), pl.ds(k * 128, 128)] * window[j + 2 : j + 66]
+                out = out + taps[pl.ds(j, 1), pl.ds(k * 128, 128)] * gpad[k, pl.ds(base + (j + 2), 64)]
             out = out.astype(BF16).astype(F32)
             conv[pl.ds(base, 64), pl.ds(k * 128, 128)] = out
             total = total + out * out
@@ -316,7 +313,7 @@
     )
 
     def act_rows(i, carry):
-        at = pl.ds(pl.multiple_of(i * 64, 64), 64)
+        at = pl.ds(pl.multiple_of(i * 128, 128), 128)
         total = jnp.sum(squares[at] + sq_in[at], axis=-1, keepdims=True)
         gain = cgain_ref[pl.ds(pl.multiple_of(core * 512, 512), 512)].astype(F32).reshape(1, 512)
         x = conv[at] * lax.rsqrt(total / CONV + EPS) * gain
@@ -335,23 +332,24 @@
     def out_columns(n):
         return jnp.concatenate([wo[8 * n + k] for k in range(8)], axis=1)
 
+    loads[3].wait()
+    loads[4].wait()
+    step0(WG)
+    loads[2].wait()
+    step0(WQ)
     loads[0].wait()
     loads[1].wait()
     step0(WKV)
-    loads[3].wait()
-    loads[4].wait()
-    step0(WG)
+    step1(WG)
+    step1(WKV)
+    step2(WG)
+    step2(WKV)
+    step1(WQ)
+    step3(WG)
+    step3(WKV)
     loads[5].wait()
     lax.fori_loop(0, rows // 64, norm_rows, 0)
     taps[...] = taps_ref[...].astype(F32)
-    loads[2].wait()
-    step0(WQ)
-    step1(WKV)
-    step1(WG)
-    step2(WKV)
-    step1(WQ)
-    step3(WKV)
-    step2(WG)
     step2(WQ)
     step4(WKV)
     for c in range(2):
@@ -360,11 +358,10 @@
         kv[me * 2 + c, pl.ds(0, 128)] = keys_t[:, :128]
         kv[me * 2 + c, pl.ds(128, 128)] = keys_t[:, 128:]
         kv[me * 2 + c, pl.ds(256, 256)] = part[:, 128:].astype(BF16)
-    step3(WG)
+    step4(WG)
+    planes_start()
     step3(WQ)
     step0(KV)
-    step4(WG)
-    planes_start()
     step4(WQ)
     for c in range(2):
         at = pl.ds(c * half, half)
@@ -372,18 +369,18 @@
     for c in range(2):
         attend_own(c)
     step1(KV)
+    attend_group(0, 2, straight)
+    planes_forward(0)
+    planes_forward(1)
+    loads[7].wait()
+    step0(WOB)
     loads[6].wait()
     step0(WOA)
-    attend_group(0, 2, straight)
-    loads[7].wait()
-    step0(WOB)
     attend_group(2, 2, straight)
     step2(KV)
     attend_group(0, 2, corner)
-    planes_forward(0)
-    planes_forward(1)
+    attend_group(2, 2, corner)
     step1(WOA)
-    attend_group(2, 2, corner)
     step1(WOB)
     planes_forward(2)
     planes_forward(3)
@@ -393,28 +390,28 @@
     for b in range(4):
         for w in range(2):
             plane_message(b, w, True, True).wait_recv()
-    step2(WOB)
     step2(WOA)
-    lax.fori_loop(0, rows // 256, gate_rows, 0)
+    gate_rows()
     for k in range(4):
         rim_box[0, k] = gpad[k, pl.ds(rows, 32)].astype(BF16)
     rim.start()
+    step2(WOB)
     attend_group(2, 2, knight)
-    step4(KV)
     rim.wait_recv()
-    step3(WOB)
     inside = jnp.where(me > 0, 1.0, 0.0)
     for k in range(4):
         gpad[k, pl.ds(0, 32)] = rim_box[1, k].astype(F32) * inside
 
     lax.fori_loop(0, rows // 64, conv_rows_of, 0)
     sq.start()
+    step4(KV)
+    step3(WOB)
+    step3(WOA)
     attend_group(0, 1, lambda i: (2, 2))
-    step3(WOA)
     lax.fori_loop(0, rows // 128, finish_rows, 0)
     sq.wait_recv()
-    lax.fori_loop(0, rows // 64, act_rows, 0)
     step4(WOB)
+    lax.fori_loop(0, rows // 128, act_rows, 0)
     step4(WOA)
     for n in range(2):
         outbox[n] = dot(both[theirs], out_columns(n)).astype(BF16)

time: 99.6 us -> 96.6 us (0.970)
  Pallas kernels: 95.9 us -> 92.8 us
    pallas_call x1, Pallas kernels: 95.9 us -> 92.8 us  [body(): pl.pallas_call(kernel, out_shape=(jax.ShapeDtypeStruct((rows // 2, d), BF...]
where the time goes in v4:
time: 96.6 us; the launch traced here: 96.4 us
  Pallas kernels  92.8 us (96%)
  local copies, waits for them, and re-layouts  2.92 us (3%)
    pallas_call x1, Pallas kernels, body(): pl.pallas_call(kernel, out_shape=(jax.ShapeDtypeStruct((rows // 2, d), BF...  92.8 us
    unnamed x4, local copies, waits for them, and re-layouts  2.92 us

profile of v4, /device:TPU:1, one launch (start us, length us, event | category | flops | bytes accessed | tf_op | source)
XLA Modules:
  0.0 96.4 jit_solution(11864116142209808274)
XLA Ops:
  0.6 92.8 %shard_map.131 = (bf16[256,2048]{1,0:T(8,128)(2,1)}, f32[8,512]{1,0:T(8,128)}) custom-call(bf16[512,2048]{1,0:T(8,128)(2,1)} %tok_hbm.1, bf16[2048]{0:T(1024)(128)(2,1)} %ngain_ref.1, bf16[128,512]{1,0:T(8,128)(2,1)} %wq_hbm.1, bf16[128,128]{1,0:T(8,128)(2,1)} %wk_hbm.1, bf16[128,128]{1,0:T(8,128)(2,1)} %wv_hbm.1, bf16[128,512]{1,0:T(8,128)(2,1)} %wgv_hbm.1, ...), custom_call_target="tpu_custom_call" | custom-call | tf_op jit(solution)/shard_map/pallas_call | solution.py:447
  93.5 0.0 copy-start
  93.5 2.3 %copy.16 = bf16[256,2048]{1,0:T(8,128)(2,1)} copy(bf16[256,2048]{1,0:T(8,128)(2,1)} %get-tuple-element.8) | data formatting | bytes 2097152
  95.8 0.0 copy-done
  95.8 0.6 copy.17
Async XLA Ops:
  93.5 2.3 %copy-start = (f32[8,512]{1,0:T(8,128)S(1)}, f32[8,512]{1,0:T(8,128)}, u32[]{:S(2)}) copy-start(f32[8,512]{1,0:T(8,128)} %get-tuple-element.5) | copy-start | bytes 49156

commit v5 on v4

--- a/solution.py
+++ b/solution.py
@@ -279,9 +279,9 @@
     )
 
     def finish_rows(i, carry):
-        at = pl.ds(pl.multiple_of(i * 128, 128), 128)
-        lane = lax.broadcasted_iota(jnp.int32, (128, 128), 1)
-        logs = jnp.zeros((128, 128), F32)
+        at = pl.ds(pl.multiple_of(i * 256, 256), 256)
+        lane = lax.broadcasted_iota(jnp.int32, (256, 128), 1)
+        logs = jnp.zeros((256, 128), F32)
         for h in range(4):
             t0 = jnp.sum(lsum[2 * h, at], axis=-1, keepdims=True)
             t1 = jnp.sum(lsum[2 * h + 1, at], axis=-1, keepdims=True)
@@ -408,7 +408,7 @@
     step3(WOB)
     step3(WOA)
     attend_group(0, 1, lambda i: (2, 2))
-    lax.fori_loop(0, rows // 128, finish_rows, 0)
+    lax.fori_loop(0, rows // 256, finish_rows, 0)
     sq.wait_recv()
     step4(WOB)
     lax.fori_loop(0, rows // 128, act_rows, 0)

time: 96.6 us -> 96.5 us (level)
  no operation moved by 1% of the time
where the time goes in v5:
time: 96.5 us; the launch traced here: 96.2 us
  Pallas kernels  92.6 us (96%)
  local copies, waits for them, and re-layouts  2.92 us (3%)
    pallas_call x1, Pallas kernels, body(): pl.pallas_call(kernel, out_shape=(jax.ShapeDtypeStruct((rows // 2, d), BF...  92.6 us
    unnamed x4, local copies, waits for them, and re-layouts  2.92 us

profile of v5, /device:TPU:1, one launch (start us, length us, event | category | flops | bytes accessed | tf_op | source)
XLA Modules:
  0.0 96.2 jit_solution(10339578555761741111)
XLA Ops:
  0.6 92.6 %shard_map.131 = (bf16[256,2048]{1,0:T(8,128)(2,1)}, f32[8,512]{1,0:T(8,128)}) custom-call(bf16[512,2048]{1,0:T(8,128)(2,1)} %tok_hbm.1, bf16[2048]{0:T(1024)(128)(2,1)} %ngain_ref.1, bf16[128,512]{1,0:T(8,128)(2,1)} %wq_hbm.1, bf16[128,128]{1,0:T(8,128)(2,1)} %wk_hbm.1, bf16[128,128]{1,0:T(8,128)(2,1)} %wv_hbm.1, bf16[128,512]{1,0:T(8,128)(2,1)} %wgv_hbm.1, ...), custom_call_target="tpu_custom_call" | custom-call | tf_op jit(solution)/shard_map/pallas_call | solution.py:447
  93.3 0.0 copy-start
  93.3 2.3 %copy.16 = bf16[256,2048]{1,0:T(8,128)(2,1)} copy(bf16[256,2048]{1,0:T(8,128)(2,1)} %get-tuple-element.8) | data formatting | bytes 2097152
  95.6 0.0 copy-done
  95.6 0.6 copy.17
Async XLA Ops:
  93.3 2.3 %copy-start = (f32[8,512]{1,0:T(8,128)S(1)}, f32[8,512]{1,0:T(8,128)}, u32[]{:S(2)}) copy-start(f32[8,512]{1,0:T(8,128)} %get-tuple-element.5) | copy-start | bytes 49156
